TPU v7x, 256 devices: a whole 4x4x8 slice. The times are simulated.
256 devices in a mesh: sp: 64 (over z, x, core), tp: 4 (over y).
Axes of the slice: x: 4, y: 4, z: 8, core: 2. Of those that a mesh axis runs over, the one named last changes fastest.
Arguments:
- hidden_in: bfloat16 [4096, 2048], P(('sp', 'tp')), may hold values from -6 to 6
- pre_gain: float32 [2048], replicated, may hold values from 0.5 to 1.5
- w_query: bfloat16 [2048, 1024], P(None, 'tp'), may hold values from -0.4375 to 0.4375
- w_key: bfloat16 [2048, 1024], P(None, 'tp'), may hold values from -0.125 to 0.125
- w_value: bfloat16 [2048, 1024], P(None, 'tp'), may hold values from -0.125 to 0.125
- stick_offset: float32 [8], P('tp'), may hold values from -15.2 to -14.2
- w_glu_a: bfloat16 [2048, 1024], P(None, 'tp'), may hold values from -0.125 to 0.125
- w_glu_b: bfloat16 [2048, 1024], P(None, 'tp'), may hold values from -0.125 to 0.125
- w_gate_attn: bfloat16 [2048, 2048], P(None, 'tp'), may hold values from -0.125 to 0.125
- w_gate_conv: bfloat16 [2048, 2048], P(None, 'tp'), may hold values from -0.125 to 0.125
- conv_taps: float32 [31, 1024], P(None, 'tp'), may hold values from -1 to 1
- conv_bias: float32 [1024], P('tp'), may hold values from -0.6 to 0.6
- norm_gain: float32 [1024], P('tp'), may hold values from 0.5 to 1.5
- norm_shift: float32 [1024], P('tp'), may hold values from -0.6 to 0.6
- w_attn_out: bfloat16 [1024, 2048], P('tp'), may hold values from -0.4375 to 0.4375
- w_conv_out: bfloat16 [1024, 2048], P('tp'), may hold values from -0.1875 to 0.1875
- post_gain: float32 [2048], P('tp'), may hold values from 0.5 to 1.5
Outputs:
- mixed: bfloat16 [4096, 2048], P('sp', 'tp')
All inputs are finite; a program needn't handle non-finite values.
Results may differ from a plain program's by a relative error of at most 0.015.
Values may be sent and summed in bfloat16 or wider, within the bound.
A program may use at most 64 MiB of HBM per device.

v0:
```python
from functools import partial
import math

import jax
import jax.numpy as jnp
from jax import lax
from jax.sharding import Mesh
from jax.sharding import PartitionSpec as P

D = 2048
HEAD_DIM = 128
CONV_CH = 1024
WIDTH = 31
SP = ("sp_0", "sp_1", "sp_2")
SP_TP = ("sp_0", "sp_1", "sp_2", "tp")


epsilon = 1e-06


def laid_out(parts, dim):
    parts = jnp.moveaxis(parts, 0, dim)
    lengths = parts.shape
    return parts.reshape(*lengths[:dim], lengths[dim] * lengths[dim + 1], *lengths[dim + 2 :])


def all_blocks(x, axes, sequence):
    parts = x[None]
    for k in sequence:
        parts = lax.all_gather(parts, axes[k], axis=0, tiled=True)
    block = [lax.axis_size(axes[k]) for k in reversed(sequence)]
    parts = parts.reshape(*block, *x.shape)
    turned = sorted(range(len(sequence)), key=lambda place: sequence[len(sequence) - 1 - place])
    return parts.transpose(*turned, *range(len(sequence), parts.ndim)).reshape(-1, *x.shape)


def whole_of(x, axes, sequence, dim):
    return laid_out(all_blocks(x, axes, sequence), dim)


def shortened(x):
    def short(part):
        return part.astype(jnp.bfloat16) if part.dtype == jnp.float32 else part

    return jax.tree.map(short, x)


def shifted(block, axis, distance):
    devices = range(lax.axis_size(axis))
    route = [(i - distance, i) for i in devices if i - distance in devices]
    return lax.ppermute(block, axis, route)


def over_pieces(x, axis):
    return lax.all_gather(x, axis).sum(0)


def own_rows(portion, extent, axis):
    count = extent * lax.axis_size(axis)
    sent = portion(jnp.int32(0), count).astype(jnp.bfloat16)
    return lax.psum_scatter(sent, axis, scatter_dimension=0, tiled=True).astype(jnp.float32)


def stick_terms(query_heads, key_block, offsets, causal):
    scores = jnp.einsum("thd,shd->hts", query_heads, key_block, preferred_element_type=jnp.float32)
    scores = scores / math.sqrt(HEAD_DIM) + offsets[:, None, None]
    log_rest = jnp.where(causal[None], jax.nn.log_sigmoid(-scores), 0.0)
    inside = lax.cumsum(log_rest, axis=2, reverse=True) - log_rest
    return (scores, log_rest, inside)


def weighted_values(scores, inside, outside, causal, value_block):
    weights = jnp.where(causal[None], jnp.exp(jax.nn.log_sigmoid(scores) + inside + outside), 0.0)
    return jnp.einsum(
        "hts,shd->thd", weights, value_block.astype(jnp.float32), precision=lax.Precision.DEFAULT
    )


def term_for(matrix, activations, offset, length):
    columns = lax.dynamic_slice_in_dim(matrix, offset, length, 1)
    return lax.dot_general(
        columns, activations, (((0,), (1,)), ((), ())), preferred_element_type=jnp.float32
    )


def held_bf16(values):
    return lax.optimization_barrier(values.astype(jnp.bfloat16))


def on_device(
    hidden_in,
    pre_gain,
    w_query,
    w_key,
    w_value,
    stick_offset,
    w_glu_a,
    w_glu_b,
    w_gate_attn,
    w_gate_conv,
    conv_taps,
    conv_bias,
    norm_gain,
    norm_shift,
    w_attn_out,
    w_conv_out,
    post_gain,
):
    weight_list = (w_query, w_key, w_value, w_glu_a, w_glu_b, w_gate_attn, w_gate_conv)

    def project(portion):
        values = portion.astype(jnp.float32)
        inverse = lax.rsqrt(jnp.mean(values * values, axis=1, keepdims=True) + epsilon)
        normed = (values * inverse * pre_gain).astype(jnp.bfloat16)
        return jnp.concatenate(
            [
                jnp.dot(normed, weight, preferred_element_type=jnp.float32).astype(jnp.bfloat16)
                for weight in weight_list
            ],
            axis=1,
        )

    joined = lax.optimization_barrier(project(lax.all_gather(hidden_in, "tp", axis=0, tiled=True)))
    pieces_list = []
    cursor = 0
    for weight in weight_list:
        pieces_list.append(joined[:, cursor : cursor + weight.shape[1]])
        cursor = cursor + weight.shape[1]
    queries, key_rows, value_rows, glu_left, glu_right, gate_attn, gate_conv = pieces_list
    row_count = joined.shape[0]
    head_count = stick_offset.shape[0]
    my_index = lax.axis_index(SP)
    local_iota = jnp.arange(row_count, dtype=jnp.int32)
    query_pos = my_index * row_count + local_iota
    query_heads = queries.reshape(row_count, head_count, HEAD_DIM)
    block_count = lax.axis_size(SP)

    def collect(running, shards, offset):
        tables, partials = running
        key_piece, value_piece = shards
        piece_blocks = key_piece.shape[0] // row_count
        key_split = key_piece.reshape(piece_blocks, row_count, head_count, HEAD_DIM)
        value_split = value_piece.reshape(piece_blocks, row_count, head_count, HEAD_DIM)
        first_block = offset // row_count

        def one_block(inputs):
            key_block, value_block, block_index = inputs
            key_pos = block_index * row_count + local_iota
            causal = key_pos[None, :] < query_pos[:, None]
            scores, log_rest, inside = stick_terms(query_heads, key_block, stick_offset, causal)
            return (
                jnp.sum(log_rest, axis=2),
                weighted_values(scores, inside, 0.0, causal, value_block),
            )

        block_ids = first_block + jnp.arange(piece_blocks, dtype=jnp.int32)
        new_sums, new_parts = lax.map(one_block, (key_split, value_split, block_ids))
        tables = lax.dynamic_update_slice_in_dim(tables, new_sums, first_block, 0)
        partials = lax.dynamic_update_slice_in_dim(partials, new_parts, first_block, 0)
        return (tables, partials)

    initial = (
        jnp.zeros((block_count, head_count, row_count), jnp.float32),
        jnp.zeros((block_count, row_count, head_count, HEAD_DIM), jnp.float32),
    )
    tables, partials = collect(
        initial,
        (
            whole_of(shortened(key_rows), SP, (1, 0, 2), 0),
            whole_of(shortened(value_rows), SP, (1, 0, 2), 0),
        ),
        jnp.int32(0),
    )
    outside = lax.cumsum(tables, axis=0, reverse=True) - tables
    summed = jnp.einsum(
        "bht,bthd->thd", jnp.exp(outside), partials, precision=lax.Precision.DEFAULT
    )
    attended = summed.reshape(row_count, head_count * HEAD_DIM).astype(jnp.bfloat16)
    gated_in = held_bf16(
        glu_left.astype(jnp.float32) * jax.nn.sigmoid(glu_right.astype(jnp.float32))
    )
    before = shifted(gated_in[row_count - (WIDTH - 1) :], SP, 1)
    padded = jnp.concatenate([before, gated_in], axis=0).astype(jnp.float32)
    channels = gated_in.shape[1]
    convolved = (
        lax.conv_general_dilated(
            padded[None],
            conv_taps.reshape(WIDTH, 1, channels),
            (1,),
            "VALID",
            dimension_numbers=("NWC", "WIO", "NWC"),
            feature_group_count=channels,
            precision=lax.Precision.DEFAULT,
        )[0]
        + conv_bias
    )
    mean_row = lax.psum(jnp.sum(convolved, axis=1), "tp") / CONV_CH
    centered = convolved - mean_row[:, None]
    spread = over_pieces(jnp.sum(centered * centered, axis=1), "tp") / CONV_CH
    conv_normed = jax.nn.silu(
        centered * lax.rsqrt(spread + epsilon)[:, None] * norm_gain + norm_shift
    ).astype(jnp.bfloat16)
    out_cols = post_gain.shape[0]
    attn_sum = own_rows(partial(term_for, w_attn_out, attended), out_cols, "tp")
    conv_sum = own_rows(partial(term_for, w_conv_out, conv_normed), out_cols, "tp")
    attn_branch = held_bf16(jnp.transpose(attn_sum)).astype(jnp.float32)
    conv_branch = held_bf16(jnp.transpose(conv_sum)).astype(jnp.float32)
    merged = (
        jax.nn.sigmoid(gate_attn.astype(jnp.float32)) * attn_branch
        + jax.nn.sigmoid(gate_conv.astype(jnp.float32)) * conv_branch
    )
    squares = lax.psum(jnp.sum(merged * merged, axis=1), "tp")
    return (merged * lax.rsqrt(squares / D + epsilon)[:, None] * post_gain).astype(jnp.bfloat16)


def solution(mesh):
    torus = Mesh(mesh.devices.reshape(8, 4, 2, mesh.shape["tp"]), ("sp_0", "sp_1", "sp_2", "tp"))
    return jax.shard_map(
        on_device,
        mesh=torus,
        in_specs=(
            P(SP_TP, None),
            P(),
            P(None, "tp"),
            P(None, "tp"),
            P(None, "tp"),
            P("tp"),
            P(None, "tp"),
            P(None, "tp"),
            P(None, "tp"),
            P(None, "tp"),
            P(None, "tp"),
            P("tp"),
            P("tp"),
            P("tp"),
            P("tp", None),
            P("tp", None),
            P("tp"),
        ),
        out_specs=P(SP, "tp"),
        check_vma=False,
    )
```

profile of v0, /device:TPU:192, one launch (start us, length us, event | category | flops | bytes accessed | tf_op | source)
XLA Modules:
  0.0 629.8 jit_solution(6772323753561475049)
XLA Ops:
  7.4 13.1 %all_gather.27 = bf16[64,2048]{1,0:T(8,128)(2,1)S(1)} all-gather(bf16[16,2048]{1,0:T(8,128)(2,1)} %param.19), channel_id=1, replica_groups=mesh['sp_0'=8,'sp_1'=4,'sp_2'=2,'tp'=4] {'tp'}, dimensions={0}, use_global_device_ids=true | all-gather | bytes 327680 | tf_op jit(solution)/shard_map/all_gather | solution.py:123
  26.9 13.2 %all-gather = bf16[256,256]{1,0:T(8,128)(2,1)} all-gather(bf16[64,256]{1,0:T(8,128)(2,1)S(1)} %get-tuple-element.199), channel_id=2, replica_groups=mesh['sp_0'=8,'sp_1'=4,'sp_2'=2,'tp'=4] {'sp_1'}, dimensions={0}, use_global_device_ids=true | all-gather | bytes 163840 | tf_op jit(solution)/shard_map/all_gather | solution.py:30
  40.2 12.7 %all-gather.1 = bf16[256,256]{1,0:T(8,128)(2,1)} all-gather(bf16[64,256]{1,0:T(8,128)(2,1)S(1)} %get-tuple-element.197), channel_id=3, replica_groups=mesh['sp_0'=8,'sp_1'=4,'sp_2'=2,'tp'=4] {'sp_1'}, dimensions={0}, use_global_device_ids=true | all-gather | bytes 163840 | tf_op jit(solution)/shard_map/all_gather | solution.py:30
  53.0 22.8 %all-gather.8.cloned.1.call-done = bf16[32,64,256]{2,1,0:T(8,128)(2,1)} async-done(((bf16[4,64,256]{2,1,0:T(8,128)(2,1)}), bf16[32,64,256]{2,1,0:T(8,128)(2,1)}) %all-gather.8.cloned.1.call-update) | async-done | bytes 1048592 | tf_op jit(solution)/shard_map/all_gather | solution.py:30
  75.8 38.9 %all-gather.12.cloned.1.call-done = bf16[32,64,256]{2,1,0:T(8,128)(2,1)} async-done(((bf16[4,64,256]{2,1,0:T(8,128)(2,1)}), bf16[32,64,256]{2,1,0:T(8,128)(2,1)}) %all-gather.12.cloned.1.call-update) | async-done | bytes 1048592 | tf_op jit(solution)/shard_map/all_gather | solution.py:30
  118.8 3.3 collective-permute-done
  124.7 10.5 %psum.14 = f32[64]{0:T(128)S(1)} all-reduce(f32[64]{0:T(128)S(1)} %fusion.40), channel_id=1, replica_groups=mesh['sp_0'=8,'sp_1'=4,'sp_2'=2,'tp'=4] {'tp'}, use_global_device_ids=true, to_apply=%region_8.9 | all-reduce | flops 64 | bytes 512 | tf_op jit(solution)/shard_map/psum | solution.py:197
  136.3 7.7 %all-reduce = f32[256]{0:T(256)S(1)} all-reduce(f32[256]{0:T(256)S(1)} %dynamic-update-slice), channel_id=4, replica_groups=mesh['sp_0'=8,'sp_1'=4,'sp_2'=2,'tp'=4] {'tp'}, use_global_device_ids=true, to_apply=%add | all-reduce | flops 256 | bytes 2048
  146.0 3.2 copy.55
  149.2 4.0 reshape_reshape_reshape.6
  153.2 3.2 copy.56
  156.4 4.0 reshape_reshape_reshape.7
  160.4 424.2 %while.15 = (s32[]{:T(128)}, f32[64,2,64]{2,1,0:T(2,128)S(1)}, bf16[64,64,2,128]{3,0,2,1:T(8,128)(2,1)}, s32[64]{0:T(128)S(1)}, bf16[64,64,2,128]{3,2,1,0:T(2,12...) while((s32[]{:T(128)}, f32[64,2,64]{2,1,0:T(2,128)S(1)}, ...), condition=%wide.region_4.5_spmd.clone.clone, body=%wide.region_1.4_spmd.clone.clone.sunk | while | flops 4960259 | bytes 737205 | solution.py:157
  164.2 2.8 dynamic_update_slice.20
  217.2 2.8 dynamic_update_slice.20
  223.8 2.8 dynamic_update_slice.20
  230.4 2.8 dynamic_update_slice.20
  237.1 2.8 dynamic_update_slice.20
  243.7 2.8 dynamic_update_slice.20
  250.4 2.8 dynamic_update_slice.20
  257.0 2.8 dynamic_update_slice.20
  263.6 2.8 dynamic_update_slice.20
  323.2 2.9 dynamic_update_slice.20
  329.9 2.9 dynamic_update_slice.20
  336.5 2.9 dynamic_update_slice.20
  343.2 2.9 dynamic_update_slice.20
  349.9 2.9 dynamic_update_slice.20
  356.5 2.9 dynamic_update_slice.20
  363.2 2.9 dynamic_update_slice.20
  369.8 2.9 dynamic_update_slice.20
  482.3 2.8 dynamic_update_slice.20
  488.9 2.8 dynamic_update_slice.20
  495.5 2.8 dynamic_update_slice.20
  502.2 2.8 dynamic_update_slice.20
  508.8 2.8 dynamic_update_slice.20
  515.4 2.8 dynamic_update_slice.20
  522.0 2.8 dynamic_update_slice.20
  528.7 2.8 dynamic_update_slice.20
  535.3 2.8 dynamic_update_slice.20
  541.9 2.8 dynamic_update_slice.20
  548.5 2.8 dynamic_update_slice.20
  555.2 2.8 dynamic_update_slice.20
  561.8 2.8 dynamic_update_slice.20
  568.4 2.8 dynamic_update_slice.20
  575.1 2.8 dynamic_update_slice.20
  581.7 2.8 dynamic_update_slice.20
  588.3 24.0 %reduce-scatter.3.cloned.1.call-done = bf16[512,64]{0,1:T(8,128)(2,1)} async-done(((bf16[2048,64]{0,1:T(8,128)(2,1)}), bf16[512,64]{0,1:T(8,128)(2,1)}) %reduce-scatter.3.cloned.1.call-update) | async-done | bytes 65552 | tf_op jit(solution)/shard_map/reduce_scatter | solution.py:61
  613.4 8.5 %psum.15 = f32[64]{0:T(128)S(1)} all-reduce(f32[64]{0:T(128)S(1)} %get-tuple-element.188), channel_id=1, replica_groups=mesh['sp_0'=8,'sp_1'=4,'sp_2'=2,'tp'=4] {'tp'}, use_global_device_ids=true, to_apply=%region_13.14 | all-reduce | flops 64 | bytes 512 | tf_op jit(solution)/shard_map/psum | solution.py:212
  (809 shorter events, 307.2 us)
Async XLA Ops:
  7.4 17.8 %copy-start = (bf16[2048,512]{1,0:T(8,128)(2,1)S(1)}, bf16[2048,512]{1,0:T(8,128)(2,1)}, u32[]{:S(2)}) copy-start(bf16[2048,512]{1,0:T(8,128)(2,1)} %param.27) | copy-start | bytes 6291460
  7.4 16.7 %copy-start.7 = (f32[2048]{0:T(1024)S(1)}, f32[2048]{0:T(1024)}, u32[]{:S(2)}) copy-start(f32[2048]{0:T(1024)} %param.20) | copy-start | bytes 24580
  7.4 16.7 %copy-start.2 = (bf16[2048,256]{1,0:T(8,128)(2,1)S(1)}, bf16[2048,256]{1,0:T(8,128)(2,1)}, u32[]{:S(2)}) copy-start(bf16[2048,256]{1,0:T(8,128)(2,1)} %param.23) | copy-start | bytes 3145732
  7.4 68.4 %all-gather.8.cloned.1.call-start = ((), (), s32[]{:S(2)}) async-start(), calls=%async_computation.2 | async-start | bytes 1179648 | tf_op jit(solution)/shard_map/all_gather | solution.py:30
  20.5 3.9 copy-start.3
  22.4 2.4 copy-start.4
  24.8 1.6 copy-start.1
  40.1 74.6 %all-gather.12.cloned.1.call-start = ((), (), s32[]{:S(2)}) async-start(), calls=%async_computation.4 | async-start | bytes 1179648 | tf_op jit(solution)/shard_map/all_gather | solution.py:30
  53.0 91.2 %copy-start.5 = (bf16[256,2048]{1,0:T(8,128)(2,1)S(1)}, bf16[256,2048]{1,0:T(8,128)(2,1)}, u32[]{:S(2)}) copy-start(bf16[256,2048]{1,0:T(8,128)(2,1)} %param.34) | copy-start | bytes 3145732
  53.0 93.0 %all-gather.10.cloned.1.call-start = ((), (), s32[]{:S(2)}) async-start(), calls=%async_computation.3 | async-start | bytes 3145728 | tf_op jit(solution)/shard_map/all_gather | solution.py:30
  75.8 77.4 %all-gather.14.cloned.1.call-start = ((), (), s32[]{:S(2)}) async-start(), calls=%async_computation.5 | async-start | bytes 3145728 | tf_op jit(solution)/shard_map/all_gather | solution.py:30
  114.8 473.5 %reduce-scatter.5.cloned.1.call-start = ((), (), s32[]{:S(2)}) async-start(), calls=%async_computation.7 | async-start | bytes 327680 | tf_op jit(solution)/shard_map/reduce_scatter | solution.py:61
  114.9 7.3 %collective-permute-start = (bf16[30,256]{1,0:T(8,128)(2,1)S(1)}, bf16[30,256]{1,0:T(8,128)(2,1)}, u32[]{:S(2)}, u32[]{:S(2)}) collective-permute-start(bf16[30,256]{1,0:T(8,128)(2,1)S(1)} %slice.39), channel_id=1, source_target_pairs={{0,4},{4,8},{8,12},{12,16},{16,20},{20,24},{24,28},{28,32},{32,36}... | collective-permute-start | bytes 46088 | tf_op jit(solution)/shard_map/ppermute | solution.py:51
  145.9 466.4 %reduce-scatter.3.cloned.1.call-start = ((), (), s32[]{:S(2)}) async-start(), calls=%async_computation.6 | async-start | bytes 327680 | tf_op jit(solution)/shard_map/reduce_scatter | solution.py:61
  156.4 4.0 copy-start.8
  156.4 4.0 copy-start.10
  584.5 2.7 copy-start.6
  585.0 37.0 %copy-start.9 = (f32[512]{0:T(512)S(1)}, f32[512]{0:T(512)}, u32[]{:S(2)}) copy-start(f32[512]{0:T(512)} %param.35) | copy-start | bytes 6148
Sparse Core Ops, SparseCore 0:
  40.3 35.4 all-gather.7
  77.6 37.1 all-gather.11
  116.5 16.9 all-gather.9
  135.2 17.1 all-gather.13
Sparse Core Ops, SparseCore 1:
  146.0 22.2 reduce-scatter.4
  588.4 23.9 reduce-scatter.2
where the time goes:
time: 639 us; the launch traced here: 630 us
  local copies, waits for them, and re-layouts  302 us (47%)
  waiting for transfers between devices  89.2 us (14%)
  other arithmetic  67.8 us (11%)
  blocking collectives  65.8 us (10%)
  loops' own time  44.3 us (7%)
  matrix products  42.6 us (7%)
  between operations  15.5 us (2%)
    dynamic_update_slice x192, local copies, waits for them, and re-layouts, collect(): lax.map(one_block, (key_split, value_split, block_ids))  185 us
    dynamic_slice x128, local copies, waits for them, and re-layouts, collect(): lax.map(one_block, (key_split, value_split, block_ids))  90.2 us
    all_gather x4, waiting for transfers between devices, all_blocks(): parts = lax.all_gather(parts, axes[k], axis=0, tiled=True)  61.7 us
    another operation x64, other arithmetic, stick_terms(): inside = lax.cumsum(log_rest, axis=2, reverse=True) - log_rest  57.8 us
    another operation x1, loops' own time, collect(): lax.map(one_block, (key_split, value_split, block_ids))  44.3 us
    all_gather x2, blocking collectives, all_blocks(): parts = lax.all_gather(parts, axes[k], axis=0, tiled=True)  25.9 us
    reduce_scatter x2, waiting for transfers between devices, own_rows(): lax.psum_scatter(sent, axis, scatter_dimension=0, tiled=True)  24.1 us
    dot_general x64, matrix products, weighted_values(): jnp.einsum('hts,shd->thd', weights, value_block.astype(jnp.float32), prec...  18.3 us
  transfers between devices with their start and end apart: 7, of which 4 were waited for; matrix products, arithmetic and copies ran while one was open for 64% of the time, Pallas kernels for 0%

commit v1 on v0

v1 whole, which is shorter than its diff:
```python
import functools
import math

import jax
import jax.numpy as jnp
from jax import lax
from jax.experimental import pallas as pl
from jax.experimental.pallas import tpu as pltpu
from jax.sharding import Mesh
from jax.sharding import PartitionSpec as P

D = 2048
HD = 128
CONV_CH = 1024
WIDTH = 31
EPS = 1e-06
MESH = pl.DeviceIdType.MESH
F32 = jnp.float32
BF16 = jnp.bfloat16
NX = 4
NZ = 8
NY = 4
NCHIP = NX * NZ


def dot(a, b):
    return jnp.dot(a, b, preferred_element_type=F32)


def dot_nt(a, b):
    return lax.dot_general(a, b, (((1,), (1,)), ((), ())), preferred_element_type=F32)


def sigmoid(v):
    return jax.nn.sigmoid(v)


(C_K0, C_V0, C_K1, C_V1, C_Q0, C_Q1, C_A, C_B, C_GA, C_GC, C_CO, C_AO) = range(12)


def kernel(
    hidden, pre_gain, w_query, w_key, w_value, offset, w_a, w_b, w_ga, w_gc,
    taps, bias, ngain, nshift, w_ao, w_co, post_gain,
    out,
    hbuf, wkv_own, wkv_oth, wq, wa, wb, wga, wgc, wco, wo,
    kvbuf, kvst, qbuf, qst, obuf, tbuf, tri,
    gst, halo, gbuf, cst, crx, stx, srx, convb, gateb, att, abuf, ssx, ssr,
    lsem, h_s, h_r, p_s, p_r, kx_s, kz_s, k_r, halo_s, halo_r,
    w_s, w_r, st_s, st_r, c_s, c_r, a_s, a_r, ss_s, ss_r,
):
    z = lax.axis_index("z")
    x = lax.axis_index("x")
    c = lax.axis_index("c")
    y = lax.axis_index("y")
    chip = z * NX + x
    oc = 1 - c

    def dev(zz=z, xx=x, cc=c, yy=y):
        return (zz, xx, cc, yy)

    def ypeer(d):
        return lax.rem(y + d, NY)

    def xpeer(d):
        return lax.rem(x + d, NX)

    def zpeer(d):
        return lax.rem(z + d + NZ, NZ)

    def rc(src, dst, ss, rs, to):
        return pltpu.make_async_remote_copy(
            src_ref=src, dst_ref=dst, send_sem=ss, recv_sem=rs, device_id=to, device_id_type=MESH
        )

    sends = []

    def start(copy):
        copy.start()
        sends.append(copy)

    own_cols = pl.ds(pl.multiple_of(c * HD, HD), HD)
    oth_cols = pl.ds(pl.multiple_of(oc * HD, HD), HD)
    lo, hi = pl.ds(0, HD), pl.ds(HD, HD)
    ycols = pl.ds(pl.multiple_of(y * 512, 512), 512)
    yrows = pl.ds(pl.multiple_of(y * 256, 256), 256)
    local = {
        C_K1: (w_key.at[:, oth_cols], wkv_oth.at[:, lo]),
        C_V1: (w_value.at[:, oth_cols], wkv_oth.at[:, hi]),
        C_K0: (w_key.at[:, own_cols], wkv_own.at[:, lo]),
        C_V0: (w_value.at[:, own_cols], wkv_own.at[:, hi]),
        C_Q1: (w_query.at[:, oth_cols], wq.at[:, hi]),
        C_Q0: (w_query.at[:, own_cols], wq.at[:, lo]),
        C_A: (w_a, wa),
        C_B: (w_b, wb),
        C_GA: (w_ga, wga),
        C_GC: (w_gc, wgc),
        C_CO: (w_co, wco),
        C_AO: (w_ao.at[:, ycols], wo.at[yrows, :]),
    }
    local = {k: pltpu.make_async_copy(s, d, lsem.at[k]) for k, (s, d) in local.items()}
    for copy in local.values():
        copy.start()

    barrier = pltpu.get_barrier_semaphore()
    next_chip = lax.rem(chip + 1, NCHIP)
    prev_chip = lax.rem(chip + NCHIP - 1, NCHIP)
    pair_chip = c * next_chip + oc * prev_chip
    pz, px = pair_chip // NX, lax.rem(pair_chip, NX)
    greet = [dev(yy=ypeer(d)) for d in (1, 2, 3)]
    greet += [dev(cc=oc, yy=ypeer(d)) for d in (0, 1, 2, 3)]
    greet += [dev(xx=xpeer(d)) for d in (1, 2, 3)]
    greet += [dev(zz=zpeer(1)), dev(zz=zpeer(-1))]
    greet += [(pz, px, oc, y)]
    for peer in greet:
        pl.semaphore_signal(barrier, inc=1, device_id=peer, device_id_type=MESH)

    hv = hidden[...].astype(F32)
    inv = lax.rsqrt(jnp.mean(hv * hv, axis=1, keepdims=True) + EPS)
    my16 = pl.ds(pl.multiple_of(y * 16, 16), 16)
    hbuf[my16, :] = (hv * inv * pre_gain[...]).astype(BF16)

    r2 = lax.broadcasted_iota(jnp.int32, (HD, 2 * HD), 0)
    c2 = lax.broadcasted_iota(jnp.int32, (HD, 2 * HD), 1)
    tri[...] = jnp.where((r2 > c2) | (c2 >= HD), 1.0, 0.0).astype(BF16)

    pl.semaphore_wait(barrier, len(greet))

    for d in (1, 3, 2):
        start(rc(hbuf.at[my16, :], hbuf.at[my16, :], h_s.at[d], h_r.at[y], dev(yy=ypeer(d))))
    for d in (1, 3, 2):
        yy = ypeer(d)
        rows = pl.ds(pl.multiple_of(yy * 16, 16), 16)
        rc(hbuf.at[rows, :], hbuf.at[rows, :], h_s.at[d], h_r.at[yy], dev(yy=yy)).wait_recv()

    my64 = pl.ds(pl.multiple_of(c * 64, 64), 64)
    oth64 = pl.ds(pl.multiple_of(oc * 64, 64), 64)
    partner = dev(cc=oc)
    local[C_K1].wait()
    local[C_V1].wait()
    kvst[...] = dot(hbuf[...], wkv_oth[...]).astype(BF16)
    start(rc(kvst, kvbuf.at[chip, my64, :], p_s.at[0], p_r.at[0], partner))
    local[C_K0].wait()
    local[C_V0].wait()
    kvbuf[chip, my64, :] = dot(hbuf[...], wkv_own[...]).astype(BF16)
    rc(kvst, kvbuf.at[chip, oth64, :], p_s.at[0], p_r.at[0], partner).wait_recv()

    def chunk_copy(idx, ss, to):
        return rc(kvbuf.at[idx], kvbuf.at[idx], ss, k_r.at[idx], to)

    for d in (1, 3, 2):
        start(chunk_copy(chip, kx_s.at[d], dev(xx=xpeer(d))))

    def z_send(idx, k, dx, up):
        to = dev(zz=zpeer(1)) if up else dev(zz=zpeer(-1))
        start(chunk_copy(idx, kz_s.at[(k * 4 + dx) * 2 + int(up)], to))

    for up in (True, False):
        z_send(chip, 0, 0, up)

    local[C_Q0].wait()
    local[C_Q1].wait()
    qv = dot(hbuf[...], wq[...]).astype(BF16)
    qst[...] = qv[:, HD:]
    start(rc(qst, qbuf.at[my64, :], p_s.at[1], p_r.at[1], partner))
    qbuf[my64, :] = qv[:, :HD]

    def wait_chunk(idx):
        rc(kvbuf.at[idx], kvbuf.at[idx], kx_s.at[0], k_r.at[idx], partner).wait_recv()

    for dx in (1, 3, 2):
        idx = z * NX + xpeer(dx)
        wait_chunk(idx)
        for up in (True, False):
            z_send(idx, 0, dx, up)

    for d in (1, 3, 2):
        yy = ypeer(d)
        cols = pl.ds(pl.multiple_of(yy * 512, 512), 512)
        start(rc(w_ao.at[:, cols], wo.at[yrows, :], w_s.at[d], w_r.at[y], dev(yy=yy)))

    local[C_A].wait()
    local[C_B].wait()
    left = dot(hbuf[...], wa[...]).astype(BF16).astype(F32)
    right = dot(hbuf[...], wb[...]).astype(BF16).astype(F32)
    gated = (left * sigmoid(right)).astype(BF16)
    gst[...] = gated[32:, :]
    gbuf[32:, :] = gated.astype(F32)
    halo_to = ((next_chip // NX) * c + z * oc, lax.rem(next_chip, NX) * c + x * oc, oc, y)
    start(rc(gst, halo, halo_s, halo_r, halo_to))

    depth_up = (4, 4, 3, 3)
    depth_down = (3, 3, 4, 4)

    def forward(k):
        for dx in (0, 1, 3, 2):
            for up in (True, False):
                depth = (depth_up if up else depth_down)[dx]
                if k > depth:
                    continue
                idx = (zpeer(-k) if up else zpeer(k)) * NX + xpeer(dx)
                wait_chunk(idx)
                if k < depth:
                    z_send(idx, k, dx, up)

    off = offset[c]
    scale = 1.0 / math.sqrt(HD)

    def block(idx):
        kb = kvbuf[idx, :, 0:HD]
        vb = kvbuf[idx, :, HD:]
        s = dot_nt(qbuf[...], kb) * scale + off
        u = jnp.exp(-jnp.abs(s))
        one = 1.0 + u
        tail = jnp.log(one) + (u - (one - 1.0))
        soft = jnp.maximum(s, 0.0) + tail
        rows = lax.broadcasted_iota(jnp.int32, (HD, HD), 0) + chip * HD
        cols = lax.broadcasted_iota(jnp.int32, (HD, HD), 1) + idx * HD
        causal = cols < rows
        logit = s - soft
        soft = jnp.where(causal, soft, 0.0)
        top = soft.astype(BF16)
        rest = (soft - top.astype(F32)).astype(BF16)
        sums = dot(top, tri[...]) + dot(rest, tri[...])
        stick = jnp.where(causal, jnp.exp(logit - sums[:, :HD]), 0.0)
        obuf[idx] = dot(stick.astype(BF16), vb)
        tbuf[idx] = sums[:, HD:]

    def row_blocks(zz):
        @pl.when(zz <= z)
        def _():
            def body(xx, carry):
                idx = zz * NX + xx

                @pl.when(idx <= chip)
                def _():
                    block(idx)

                return carry

            lax.fori_loop(0, NX, body, 0)

    forward(1)
    local[C_GA].wait()
    local[C_GC].wait()
    gateb[0] = sigmoid(dot(hbuf[...], wga[...]).astype(BF16).astype(F32))
    gateb[1] = sigmoid(dot(hbuf[...], wgc[...]).astype(BF16).astype(F32))

    rc(qst, qbuf.at[oth64, :], p_s.at[1], p_r.at[1], partner).wait_recv()
    row_blocks(z)
    row_blocks(zpeer(-1))

    rc(gst, halo, halo_s, halo_r, halo_to).wait_recv()
    first = (chip * 2 + c) == 0
    gbuf[0:32, :] = jnp.where(first, 0.0, halo[...].astype(F32))
    conv = jnp.broadcast_to(bias[...], (64, 256))
    for i in range(WIDTH):
        conv = conv + taps[i : i + 1, :] * gbuf[2 + i : 66 + i, :]
    local_mean = jnp.mean(conv, axis=1, keepdims=True)
    dev_local = conv - local_mean
    local_m2 = jnp.sum(dev_local * dev_local, axis=1, keepdims=True)
    lane = lax.broadcasted_iota(jnp.int32, (64, HD), 1)
    stx[...] = jnp.where(lane < 64, local_mean, local_m2)
    for d in (1, 3, 2):
        start(rc(stx, srx.at[y], st_s.at[d], st_r.at[y], dev(yy=ypeer(d))))
    convb[...] = conv

    forward(2)
    row_blocks(zpeer(-2))

    srx[y] = stx[...]
    for d in (1, 3, 2):
        yy = ypeer(d)
        rc(stx, srx.at[yy], st_s.at[d], st_r.at[yy], dev(yy=yy)).wait_recv()
    stats = [srx[i] for i in range(NY)]
    means = [t[:, 0:1] for t in stats]
    mean = (means[0] + means[1] + means[2] + means[3]) * 0.25
    m2 = stats[0][:, 64:65] + stats[1][:, 64:65] + stats[2][:, 64:65] + stats[3][:, 64:65]
    for t in means:
        m2 = m2 + 256.0 * (t - mean) * (t - mean)
    cn = (convb[...] - mean) * lax.rsqrt(m2 / CONV_CH + EPS) * ngain[...] + nshift[...]
    cn = (cn * sigmoid(cn)).astype(BF16)
    local[C_CO].wait()
    for i in range(NY):
        cst[i] = dot(cn, wco[:, i * 512 : (i + 1) * 512]).astype(BF16)
    for d in (1, 3, 2):
        yy = ypeer(d)
        start(rc(cst.at[yy], crx.at[y], c_s.at[d], c_r.at[y], dev(yy=yy)))

    forward(3)
    row_blocks(zpeer(-3))
    row_blocks(zpeer(1))

    csum = cst[y].astype(F32)
    for d in (1, 3, 2):
        yy = ypeer(d)
        rc(cst.at[yy], crx.at[yy], c_s.at[d], c_r.at[yy], dev(yy=yy)).wait_recv()
        csum = csum + crx[yy].astype(F32)
    gateb[1] = gateb[1] * csum.astype(BF16).astype(F32)

    forward(4)
    row_blocks(zpeer(2))
    row_blocks(zpeer(3))
    row_blocks(zpeer(4))

    def combine(j, state):
        acc, carry = state
        idx = chip - j
        return (acc + obuf[idx] * jnp.exp(-carry), carry + tbuf[idx])

    zero = jnp.zeros((HD, HD), F32)
    acc, _ = lax.fori_loop(0, chip + 1, combine, (zero, zero))
    att[...] = acc.astype(BF16)

    head = pl.ds(pl.multiple_of((y * 2 + c) * HD, HD), HD)
    n = 0
    for d in (0, 1, 3, 2):
        for cc, rows in ((c, my64), (oc, oth64)):
            if d == 0 and cc is c:
                continue
            start(rc(att.at[rows, :], abuf.at[:, head], a_s.at[n], a_r.at[y * 2 + c], dev(cc=cc, yy=ypeer(d))))
            n += 1
    abuf[:, head] = att[my64, :]
    local[C_AO].wait()
    for d in (1, 3, 2):
        yy = ypeer(d)
        rows = pl.ds(pl.multiple_of(yy * 256, 256), 256)
        rc(w_ao.at[:, ycols], wo.at[rows, :], w_s.at[d], w_r.at[yy], dev(yy=yy)).wait_recv()
    for d in (0, 1, 3, 2):
        for cc in (c, oc):
            if d == 0 and cc is c:
                continue
            yy = ypeer(d)
            h = yy * 2 + cc
            cols = pl.ds(pl.multiple_of(h * HD, HD), HD)
            rc(att.at[my64, :], abuf.at[:, cols], a_s.at[0], a_r.at[h], dev(cc=oc, yy=yy)).wait_recv()
    branch = dot(abuf[...], wo[...]).astype(BF16).astype(F32)
    merged = gateb[0] * branch + gateb[1]
    sq = merged * merged
    part = sq[:, 0:128] + sq[:, 128:256] + sq[:, 256:384] + sq[:, 384:512]
    part = jnp.concatenate([part, jnp.zeros((64, HD), F32)], axis=0).T
    ssx[...] = jnp.sum(part.reshape(16, 8, HD), axis=0)
    for d in (1, 3, 2):
        start(rc(ssx, ssr.at[y], ss_s.at[d], ss_r.at[y], dev(yy=ypeer(d))))
    total = ssx[...]
    for d in (1, 3, 2):
        yy = ypeer(d)
        rc(ssx, ssr.at[yy], ss_s.at[d], ss_r.at[yy], dev(yy=yy)).wait_recv()
        total = total + ssr[yy]
    total = jnp.broadcast_to(jnp.sum(total, axis=0, keepdims=True), (HD, HD)).T[:64, 0:1]
    out[...] = (merged * lax.rsqrt(total / D + EPS) * post_gain[...]).astype(BF16)

    for copy in sends:
        copy.wait_send()


def on_device(
    hidden_in, pre_gain, w_query, w_key, w_value, stick_offset, w_glu_a, w_glu_b, w_gate_attn,
    w_gate_conv, conv_taps, conv_bias, norm_gain, norm_shift, w_attn_out, w_conv_out, post_gain,
):
    vm = pl.BlockSpec(memory_space=pltpu.VMEM)
    hb = pl.BlockSpec(memory_space=pl.ANY)
    sm = pl.BlockSpec(memory_space=pltpu.SMEM)
    dma = pltpu.SemaphoreType.DMA
    return pl.pallas_call(
        kernel,
        out_shape=jax.ShapeDtypeStruct((64, 512), BF16),
        in_specs=[vm, vm, hb, hb, hb, sm, hb, hb, hb, hb, vm, vm, vm, vm, hb, hb, vm],
        out_specs=vm,
        scratch_shapes=[
            pltpu.VMEM((64, D), BF16),
            pltpu.VMEM((D, 256), BF16),
            pltpu.VMEM((D, 256), BF16),
            pltpu.VMEM((D, 256), BF16),
            pltpu.VMEM((D, 256), BF16),
            pltpu.VMEM((D, 256), BF16),
            pltpu.VMEM((D, 512), BF16),
            pltpu.VMEM((D, 512), BF16),
            pltpu.VMEM((256, D), BF16),
            pltpu.VMEM((1024, 512), BF16),
            pltpu.VMEM((NCHIP, 128, 256), BF16),
            pltpu.VMEM((64, 256), BF16),
            pltpu.VMEM((128, 128), BF16),
            pltpu.VMEM((64, 128), BF16),
            pltpu.VMEM((NCHIP, 128, 128), F32),
            pltpu.VMEM((NCHIP, 128, 128), F32),
            pltpu.VMEM((128, 256), BF16),
            pltpu.VMEM((32, 256), BF16),
            pltpu.VMEM((32, 256), BF16),
            pltpu.VMEM((96, 256), F32),
            pltpu.VMEM((NY, 64, 512), BF16),
            pltpu.VMEM((NY, 64, 512), BF16),
            pltpu.VMEM((64, 128), F32),
            pltpu.VMEM((NY, 64, 128), F32),
            pltpu.VMEM((64, 256), F32),
            pltpu.VMEM((2, 64, 512), F32),
            pltpu.VMEM((128, 128), BF16),
            pltpu.VMEM((64, 1024), BF16),
            pltpu.VMEM((8, 128), F32),
            pltpu.VMEM((NY, 8, 128), F32),
            dma((12,)),
            dma((4,)), dma((4,)),
            dma((2,)), dma((2,)),
            dma((4,)), dma((40,)), dma((NCHIP,)),
            dma, dma,
            dma((4,)), dma((4,)),
            dma((4,)), dma((4,)),
            dma((4,)), dma((4,)),
            dma((7,)), dma((8,)),
            dma((4,)), dma((4,)),
        ],
        compiler_params=pltpu.CompilerParams(
            collective_id=0, has_side_effects=True, vmem_limit_bytes=56 * 1024 * 1024
        ),
    )(
        hidden_in, pre_gain.reshape(1, -1), w_query, w_key, w_value, stick_offset, w_glu_a,
        w_glu_b, w_gate_attn, w_gate_conv, conv_taps, conv_bias.reshape(1, -1),
        norm_gain.reshape(1, -1), norm_shift.reshape(1, -1), w_attn_out, w_conv_out,
        post_gain.reshape(1, -1),
    )


def solution(mesh):
    torus = Mesh(mesh.devices.reshape(NZ, NX, 2, NY), ("z", "x", "c", "y"))
    every = ("z", "x", "c", "y")
    cols = P(None, "y")
    return jax.shard_map(
        on_device,
        mesh=torus,
        in_specs=(
            P(every, None), P(), cols, cols, cols, P("y"), cols, cols, cols, cols, cols,
            P("y"), P("y"), P("y"), P("y", None), P("y", None), P("y"),
        ),
        out_specs=P(("z", "x", "c"), "y"),
        check_vma=False,
    )
```

time: 639 us -> 58.8 us (0.09)
  the two profiles are of different devices: /device:TPU:192 before, /device:TPU:230 now
where the time goes in v1:
time: 58.8 us; the launch traced here: 58.7 us
  Pallas kernels  57.2 us (97%)
  local copies, waits for them, and re-layouts  1.47 us (2%)
    pallas_call x1, Pallas kernels, on_device(): pl.pallas_call(kernel, out_shape=jax.ShapeDtypeStruct((64, 512), BF16), i...  57.2 us
    unnamed x1, local copies, waits for them, and re-layouts  1.47 us

profile of v1, /device:TPU:230, one launch (start us, length us, event | category | flops | bytes accessed | tf_op | source)
XLA Modules:
  0.0 58.7 jit_solution(15354376359718797653)
XLA Ops:
  0.0 57.2 %shard_map.163 = bf16[64,512]{1,0:T(8,128)(2,1)} custom-call(bf16[16,2048]{1,0:T(8,128)(2,1)} %hidden.1, f32[1,2048]{1,0:T(1,128)} %bitcast.5, bf16[2048,256]{1,0:T(8,128)(2,1)} %w_query.1, bf16[2048,256]{1,0:T(8,128)(2,1)} %w_key.1, bf16[2048,256]{1,0:T(8,128)(2,1)} %w_value.1, f32[2]{0:T(128)} %offset.1, bf16[2048,256]{1,0:T(8,128)(2,1)} %w_a.1, ...), custom_call_target="tpu_custom_call" | custom-call | tf_op jit(solution)/shard_map/pallas_call | solution.py:364
  57.2 1.5 %copy.19 = bf16[64,512]{1,0:T(8,128)(2,1)} copy(bf16[64,512]{1,0:T(8,128)(2,1)} %shard_map.163) | data formatting | bytes 131072

commit v2 on v1

--- a/solution.py
+++ b/solution.py
@@ -23,6 +23,40 @@
 NCHIP = NX * NZ
 
 
+ORDER0 = (
+    (0, 0), (-1, 0), (0, 1), (0, 3), (1, 0), (0, 2), (-2, 0), (1, 1),
+    (-1, 1), (1, 3), (-1, 3), (2, 0), (-1, 2), (1, 2), (-3, 0), (2, 1),
+    (-2, 1), (2, 3), (3, 0), (-2, 3), (2, 2), (-2, 2), (3, 1), (-4, 0),
+    (3, 3), (-3, 1), (-3, 3), (3, 2), (-3, 2), (4, 3), (-4, 1), (4, 2),
+)
+ORDER1 = (
+    (0, 0), (-1, 0), (0, 1), (0, 3), (1, 0), (-1, 1), (-1, 3), (-2, 0),
+    (2, 0), (0, 2), (1, 1), (1, 3), (-1, 2), (-2, 3), (-2, 1), (-3, 0),
+    (3, 0), (2, 3), (2, 1), (1, 2), (-2, 2), (-3, 1), (-3, 3), (-4, 0),
+    (3, 1), (3, 3), (2, 2), (-3, 2), (-4, 3), (-4, 1), (3, 2), (-4, 2),
+)
+UP0, DOWN0 = (4, 4, 3, 3), (3, 3, 4, 4)
+UP1, DOWN1 = 4, 3
+
+
+def hops(core, dz, dx):
+    if core == 0:
+        if dz == 0:
+            return [("z", 1), ("z", -1)] + ([("x", 1), ("x", 3), ("x", 2)] if dx == 0 else [])
+        if dz < 0:
+            return [("z", 1)] if -dz < UP0[dx] else []
+        return [("z", -1)] if dz < DOWN0[dx] else []
+    if dx == 0:
+        along = [("z", 1)] * (-UP1 < dz <= 0) + [("z", -1)] * (0 <= dz < DOWN1)
+        return along + [("x", 1), ("x", 3)]
+    if dx == 3:
+        return [("x", 1)] if dz % 2 == 0 else []
+    return [("x", 3)] if dx == 1 and dz % 2 == 1 else []
+
+
+SENDS = [sum(len(hops(core, *t)) for t in order) for core, order in ((0, ORDER0), (1, ORDER1))]
+
+
 def dot(a, b):
     return jnp.dot(a, b, preferred_element_type=F32)
 
@@ -45,7 +79,7 @@
     hbuf, wkv_own, wkv_oth, wq, wa, wb, wga, wgc, wco, wo,
     kvbuf, kvst, qbuf, qst, obuf, tbuf, tri,
     gst, halo, gbuf, cst, crx, stx, srx, convb, gateb, att, abuf, ssx, ssr,
-    lsem, h_s, h_r, p_s, p_r, kx_s, kz_s, k_r, halo_s, halo_r,
+    lsem, h_s, h_r, p_s, p_r, k_s, k_r, halo_s, halo_r,
     w_s, w_r, st_s, st_r, c_s, c_r, a_s, a_r, ss_s, ss_r,
 ):
     z = lax.axis_index("z")
@@ -119,8 +153,8 @@
     my16 = pl.ds(pl.multiple_of(y * 16, 16), 16)
     hbuf[my16, :] = (hv * inv * pre_gain[...]).astype(BF16)
 
-    r2 = lax.broadcasted_iota(jnp.int32, (HD, 2 * HD), 0)
-    c2 = lax.broadcasted_iota(jnp.int32, (HD, 2 * HD), 1)
+    r2 = lax.broadcasted_iota(jnp.int32, (2 * HD, 2 * HD), 0) % HD
+    c2 = lax.broadcasted_iota(jnp.int32, (2 * HD, 2 * HD), 1)
     tri[...] = jnp.where((r2 > c2) | (c2 >= HD), 1.0, 0.0).astype(BF16)
 
     pl.semaphore_wait(barrier, len(greet))
@@ -147,31 +181,43 @@
     def chunk_copy(idx, ss, to):
         return rc(kvbuf.at[idx], kvbuf.at[idx], ss, k_r.at[idx], to)
 
-    for d in (1, 3, 2):
-        start(chunk_copy(chip, kx_s.at[d], dev(xx=xpeer(d))))
-
-    def z_send(idx, k, dx, up):
-        to = dev(zz=zpeer(1)) if up else dev(zz=zpeer(-1))
-        start(chunk_copy(idx, kz_s.at[(k * 4 + dx) * 2 + int(up)], to))
-
-    for up in (True, False):
-        z_send(chip, 0, 0, up)
-
+    counts = [0, 0]
+
+    def send_on(core, dz, dx):
+        copies = hops(core, dz, dx)
+        if not copies:
+            return
+        first = counts[core]
+        counts[core] += len(copies)
+
+        @pl.when(c == core)
+        def _():
+            idx = zpeer(dz) * NX + xpeer(dx)
+            for i, (axis, step) in enumerate(copies):
+                to = dev(zz=zpeer(step)) if axis == "z" else dev(xx=xpeer(step))
+                chunk_copy(idx, k_s.at[first + i], to).start()
+
+    def chunk(n):
+        (z0, x0), (z1, x1) = ORDER0[n], ORDER1[n]
+        dz = z0 * oc + z1 * c
+        dx = x0 * oc + x1 * c
+        return zpeer(dz) * NX + xpeer(dx)
+
+    def arrivals(first, last):
+        for n in range(first, last):
+            if n > 0:
+                idx = chunk(n)
+                rc(kvbuf.at[idx], kvbuf.at[idx], k_s.at[0], k_r.at[idx], partner).wait_recv()
+            send_on(0, *ORDER0[n])
+            send_on(1, *ORDER1[n])
+
+    arrivals(0, 1)
     local[C_Q0].wait()
     local[C_Q1].wait()
     qv = dot(hbuf[...], wq[...]).astype(BF16)
     qst[...] = qv[:, HD:]
     start(rc(qst, qbuf.at[my64, :], p_s.at[1], p_r.at[1], partner))
     qbuf[my64, :] = qv[:, :HD]
-
-    def wait_chunk(idx):
-        rc(kvbuf.at[idx], kvbuf.at[idx], kx_s.at[0], k_r.at[idx], partner).wait_recv()
-
-    for dx in (1, 3, 2):
-        idx = z * NX + xpeer(dx)
-        wait_chunk(idx)
-        for up in (True, False):
-            z_send(idx, 0, dx, up)
 
     for d in (1, 3, 2):
         yy = ypeer(d)
@@ -188,66 +234,50 @@
     halo_to = ((next_chip // NX) * c + z * oc, lax.rem(next_chip, NX) * c + x * oc, oc, y)
     start(rc(gst, halo, halo_s, halo_r, halo_to))
 
-    depth_up = (4, 4, 3, 3)
-    depth_down = (3, 3, 4, 4)
-
-    def forward(k):
-        for dx in (0, 1, 3, 2):
-            for up in (True, False):
-                depth = (depth_up if up else depth_down)[dx]
-                if k > depth:
-                    continue
-                idx = (zpeer(-k) if up else zpeer(k)) * NX + xpeer(dx)
-                wait_chunk(idx)
-                if k < depth:
-                    z_send(idx, k, dx, up)
-
-    off = offset[c]
-    scale = 1.0 / math.sqrt(HD)
-
-    def block(idx):
-        kb = kvbuf[idx, :, 0:HD]
-        vb = kvbuf[idx, :, HD:]
-        s = dot_nt(qbuf[...], kb) * scale + off
-        u = jnp.exp(-jnp.abs(s))
-        one = 1.0 + u
-        tail = jnp.log(one) + (u - (one - 1.0))
-        soft = jnp.maximum(s, 0.0) + tail
-        rows = lax.broadcasted_iota(jnp.int32, (HD, HD), 0) + chip * HD
-        cols = lax.broadcasted_iota(jnp.int32, (HD, HD), 1) + idx * HD
-        causal = cols < rows
-        logit = s - soft
-        soft = jnp.where(causal, soft, 0.0)
-        top = soft.astype(BF16)
-        rest = (soft - top.astype(F32)).astype(BF16)
-        sums = dot(top, tri[...]) + dot(rest, tri[...])
-        stick = jnp.where(causal, jnp.exp(logit - sums[:, :HD]), 0.0)
-        obuf[idx] = dot(stick.astype(BF16), vb)
-        tbuf[idx] = sums[:, HD:]
-
-    def row_blocks(zz):
-        @pl.when(zz <= z)
-        def _():
-            def body(xx, carry):
-                idx = zz * NX + xx
-
-                @pl.when(idx <= chip)
-                def _():
-                    block(idx)
-
-                return carry
-
-            lax.fori_loop(0, NX, body, 0)
-
-    forward(1)
     local[C_GA].wait()
     local[C_GC].wait()
     gateb[0] = sigmoid(dot(hbuf[...], wga[...]).astype(BF16).astype(F32))
     gateb[1] = sigmoid(dot(hbuf[...], wgc[...]).astype(BF16).astype(F32))
-
     rc(qst, qbuf.at[oth64, :], p_s.at[1], p_r.at[1], partner).wait_recv()
-    row_blocks(z)
-    row_blocks(zpeer(-1))
+
+    off = offset[c]
+    scale = 1.0 / math.sqrt(HD)
+
+    def blocks(first, last):
+        chunks = [chunk(n) for n in range(first, last)]
+        needed = chunks[0] <= chip
+        for idx in chunks[1:]:
+            needed = needed | (idx <= chip)
+
+        @pl.when(needed)
+        def _():
+            fronts = []
+            for n, idx in enumerate(chunks, first):
+                s = dot_nt(qbuf[...], kvbuf[idx, :, 0:HD]) * scale + off
+                u = jnp.exp(-jnp.abs(s))
+                one = 1.0 + u
+                tail = jnp.log(one) + (u - (one - 1.0))
+                soft = jnp.maximum(s, 0.0) + tail
+                logit = s - soft
+                if n == 0:
+                    rows = lax.broadcasted_iota(jnp.int32, (HD, HD), 0)
+                    causal = lax.broadcasted_iota(jnp.int32, (HD, HD), 1) < rows
+                    soft = jnp.where(causal, soft, 0.0)
+                    logit = jnp.where(causal, logit, -jnp.inf)
+                top = soft.astype(BF16)
+                rest = (soft - top.astype(F32)).astype(BF16)
+                fronts.append((logit, jnp.concatenate([top, rest], axis=1)))
+            sums = [dot(pair, tri[...]) for _, pair in fronts]
+            for idx, t in zip(chunks, sums):
+                tbuf[idx] = t[:, HD:]
+            sticks = [jnp.exp(f[0] - t[:, :HD]).astype(BF16) for f, t in zip(fronts, sums)]
+            for idx, stick in zip(chunks, sticks):
+                obuf[idx] = dot(stick, kvbuf[idx, :, HD:])
+
+    arrivals(1, 4)
+    blocks(0, 4)
+    arrivals(4, 8)
+    blocks(4, 8)
 
     rc(gst, halo, halo_s, halo_r, halo_to).wait_recv()
     first = (chip * 2 + c) == 0
@@ -264,8 +294,10 @@
         start(rc(stx, srx.at[y], st_s.at[d], st_r.at[y], dev(yy=ypeer(d))))
     convb[...] = conv
 
-    forward(2)
-    row_blocks(zpeer(-2))
+    arrivals(8, 12)
+    blocks(8, 12)
+    arrivals(12, 16)
+    blocks(12, 16)
 
     srx[y] = stx[...]
     for d in (1, 3, 2):
@@ -286,9 +318,10 @@
         yy = ypeer(d)
         start(rc(cst.at[yy], crx.at[y], c_s.at[d], c_r.at[y], dev(yy=yy)))
 
-    forward(3)
-    row_blocks(zpeer(-3))
-    row_blocks(zpeer(1))
+    arrivals(16, 20)
+    blocks(16, 20)
+    arrivals(20, 24)
+    blocks(20, 24)
 
     csum = cst[y].astype(F32)
     for d in (1, 3, 2):
@@ -297,10 +330,10 @@
         csum = csum + crx[yy].astype(F32)
     gateb[1] = gateb[1] * csum.astype(BF16).astype(F32)
 
-    forward(4)
-    row_blocks(zpeer(2))
-    row_blocks(zpeer(3))
-    row_blocks(zpeer(4))
+    arrivals(24, 28)
+    blocks(24, 28)
+    arrivals(28, 32)
+    blocks(28, 32)
 
     def combine(j, state):
         acc, carry = state
@@ -351,6 +384,12 @@
 
     for copy in sends:
         copy.wait_send()
+    for i in range(max(SENDS)):
+        ended = rc(kvbuf.at[chip], kvbuf.at[chip], k_s.at[i], k_r.at[chip], partner).wait_send
+        if i < min(SENDS):
+            ended()
+        else:
+            pl.when(c == SENDS.index(max(SENDS)))(ended)
 
 
 def on_device(
@@ -383,7 +422,7 @@
             pltpu.VMEM((64, 128), BF16),
             pltpu.VMEM((NCHIP, 128, 128), F32),
             pltpu.VMEM((NCHIP, 128, 128), F32),
-            pltpu.VMEM((128, 256), BF16),
+            pltpu.VMEM((256, 256), BF16),
             pltpu.VMEM((32, 256), BF16),
             pltpu.VMEM((32, 256), BF16),
             pltpu.VMEM((96, 256), F32),
@@ -400,7 +439,7 @@
             dma((12,)),
             dma((4,)), dma((4,)),
             dma((2,)), dma((2,)),
-            dma((4,)), dma((40,)), dma((NCHIP,)),
+            dma((max(SENDS),)), dma((NCHIP,)),
             dma, dma,
             dma((4,)), dma((4,)),
             dma((4,)), dma((4,)),

time: 58.8 us -> 53.8 us (0.915)
  the two profiles are of different devices: /device:TPU:230 before, /device:TPU:1 now
where the time goes in v2:
time: 53.8 us; the launch traced here: 53.6 us
  Pallas kernels  52.1 us (97%)
  local copies, waits for them, and re-layouts  1.47 us (3%)
    pallas_call x1, Pallas kernels, on_device(): pl.pallas_call(kernel, out_shape=jax.ShapeDtypeStruct((64, 512), BF16), i...  52.1 us
    unnamed x1, local copies, waits for them, and re-layouts  1.47 us

profile of v2, /device:TPU:1, one launch (start us, length us, event | category | flops | bytes accessed | tf_op | source)
XLA Modules:
  0.0 53.6 jit_solution(3102423069067394881)
XLA Ops:
  0.0 52.1 %shard_map.163 = bf16[64,512]{1,0:T(8,128)(2,1)} custom-call(bf16[16,2048]{1,0:T(8,128)(2,1)} %hidden.1, f32[1,2048]{1,0:T(1,128)} %bitcast.5, bf16[2048,256]{1,0:T(8,128)(2,1)} %w_query.1, bf16[2048,256]{1,0:T(8,128)(2,1)} %w_key.1, bf16[2048,256]{1,0:T(8,128)(2,1)} %w_value.1, f32[2]{0:T(128)} %offset.1, bf16[2048,256]{1,0:T(8,128)(2,1)} %w_a.1, ...), custom_call_target="tpu_custom_call" | custom-call | tf_op jit(solution)/shard_map/pallas_call | solution.py:403
  52.1 1.5 %copy.19 = bf16[64,512]{1,0:T(8,128)(2,1)} copy(bf16[64,512]{1,0:T(8,128)(2,1)} %shard_map.163) | data formatting | bytes 131072

commit v3 on v2

--- a/solution.py
+++ b/solution.py
@@ -23,38 +23,25 @@
 NCHIP = NX * NZ
 
 
-ORDER0 = (
-    (0, 0), (-1, 0), (0, 1), (0, 3), (1, 0), (0, 2), (-2, 0), (1, 1),
-    (-1, 1), (1, 3), (-1, 3), (2, 0), (-1, 2), (1, 2), (-3, 0), (2, 1),
-    (-2, 1), (2, 3), (3, 0), (-2, 3), (2, 2), (-2, 2), (3, 1), (-4, 0),
-    (3, 3), (-3, 1), (-3, 3), (3, 2), (-3, 2), (4, 3), (-4, 1), (4, 2),
+ORDER = (
+    (0, 0), (7, 0), (1, 0), (6, 0), (0, 1), (0, 3), (2, 0), (5, 0),
+    (7, 1), (7, 3), (3, 0), (1, 1), (1, 3), (6, 1), (6, 3), (4, 0),
+    (2, 1), (0, 2), (5, 1), (2, 3), (7, 2), (5, 3), (3, 1), (3, 3),
+    (6, 2), (1, 2), (4, 1), (4, 3), (5, 2), (2, 2), (3, 2), (4, 2),
 )
-ORDER1 = (
-    (0, 0), (-1, 0), (0, 1), (0, 3), (1, 0), (-1, 1), (-1, 3), (-2, 0),
-    (2, 0), (0, 2), (1, 1), (1, 3), (-1, 2), (-2, 3), (-2, 1), (-3, 0),
-    (3, 0), (2, 3), (2, 1), (1, 2), (-2, 2), (-3, 1), (-3, 3), (-4, 0),
-    (3, 1), (3, 3), (2, 2), (-3, 2), (-4, 3), (-4, 1), (3, 2), (-4, 2),
-)
-UP0, DOWN0 = (4, 4, 3, 3), (3, 3, 4, 4)
-UP1, DOWN1 = 4, 3
-
-
-def hops(core, dz, dx):
-    if core == 0:
-        if dz == 0:
-            return [("z", 1), ("z", -1)] + ([("x", 1), ("x", 3), ("x", 2)] if dx == 0 else [])
-        if dz < 0:
-            return [("z", 1)] if -dz < UP0[dx] else []
-        return [("z", -1)] if dz < DOWN0[dx] else []
+UP = 4
+WRAPS = (7, 6, 5)
+
+
+def hops(k, dx):
     if dx == 0:
-        along = [("z", 1)] * (-UP1 < dz <= 0) + [("z", -1)] * (0 <= dz < DOWN1)
-        return along + [("x", 1), ("x", 3)]
+        return [("x", 1), ("x", 3)] + [("z", 1)] * (k < UP)
     if dx == 3:
-        return [("x", 1)] if dz % 2 == 0 else []
-    return [("x", 3)] if dx == 1 and dz % 2 == 1 else []
-
-
-SENDS = [sum(len(hops(core, *t)) for t in order) for core, order in ((0, ORDER0), (1, ORDER1))]
+        return [("x", 1)] if k % 2 == 0 else []
+    return [("x", 3)] if dx == 1 and k % 2 == 1 else []
+
+
+SENDS = sum(len(hops(*t)) for t in ORDER)
 
 
 def dot(a, b):
@@ -79,8 +66,8 @@
     hbuf, wkv_own, wkv_oth, wq, wa, wb, wga, wgc, wco, wo,
     kvbuf, kvst, qbuf, qst, obuf, tbuf, tri,
     gst, halo, gbuf, cst, crx, stx, srx, convb, gateb, att, abuf, ssx, ssr,
-    lsem, h_s, h_r, p_s, p_r, k_s, k_r, halo_s, halo_r,
-    w_s, w_r, st_s, st_r, c_s, c_r, a_s, a_r, ss_s, ss_r,
+    lsem, h_s, h_r, p_s, p_r, k_s, wrap_s, k_r, ready, halo_s, halo_r,
+    w_s, w_r, v_s, v_r, st_s, st_r, c_s, c_r, a_s, a_r, ss_s, ss_r,
 ):
     z = lax.axis_index("z")
     x = lax.axis_index("x")
@@ -105,6 +92,11 @@
         return pltpu.make_async_remote_copy(
             src_ref=src, dst_ref=dst, send_sem=ss, recv_sem=rs, device_id=to, device_id_type=MESH
         )
+
+    half = pl.ds(pl.multiple_of(c * HD, HD), HD)
+
+    def whalf(yy, cc):
+        return pl.ds(pl.multiple_of(yy * 256 + cc * HD, HD), HD)
 
     sends = []
 
@@ -142,11 +134,25 @@
     pz, px = pair_chip // NX, lax.rem(pair_chip, NX)
     greet = [dev(yy=ypeer(d)) for d in (1, 2, 3)]
     greet += [dev(cc=oc, yy=ypeer(d)) for d in (0, 1, 2, 3)]
-    greet += [dev(xx=xpeer(d)) for d in (1, 2, 3)]
-    greet += [dev(zz=zpeer(1)), dev(zz=zpeer(-1))]
-    greet += [(pz, px, oc, y)]
+    greet += [dev(xx=xpeer(d)) for d in (1, 3)]
     for peer in greet:
         pl.semaphore_signal(barrier, inc=1, device_id=peer, device_id_type=MESH)
+    greeted = len(greet)
+    for k in (1,) + WRAPS:
+        @pl.when(z + k < NZ)
+        def _():
+            pl.semaphore_signal(barrier, inc=1, device_id=dev(zz=zpeer(k)), device_id_type=MESH)
+
+        greeted = greeted + jnp.where(z >= k, 1, 0)
+    next_core = (pz, px, oc, y)
+    has_next = (c == 1) & (chip < NCHIP - 1)
+    has_prev = (c == 0) & (chip > 0)
+
+    @pl.when(has_next)
+    def _():
+        pl.semaphore_signal(barrier, inc=1, device_id=next_core, device_id_type=MESH)
+
+    greeted = greeted + jnp.where(has_prev, 1, 0)
 
     hv = hidden[...].astype(F32)
     inv = lax.rsqrt(jnp.mean(hv * hv, axis=1, keepdims=True) + EPS)
@@ -157,7 +163,16 @@
     c2 = lax.broadcasted_iota(jnp.int32, (2 * HD, 2 * HD), 1)
     tri[...] = jnp.where((r2 > c2) | (c2 >= HD), 1.0, 0.0).astype(BF16)
 
-    pl.semaphore_wait(barrier, len(greet))
+    pl.semaphore_wait(barrier, greeted)
+    for k in (1,) + WRAPS:
+        @pl.when(z >= k)
+        def _():
+            pl.semaphore_signal(ready.at[k], inc=1, device_id=dev(zz=zpeer(-k)), device_id_type=MESH)
+
+    @pl.when(has_prev)
+    def _():
+        pl.semaphore_signal(ready.at[0], inc=1, device_id=next_core, device_id_type=MESH)
+
 
     for d in (1, 3, 2):
         start(rc(hbuf.at[my16, :], hbuf.at[my16, :], h_s.at[d], h_r.at[y], dev(yy=ypeer(d))))
@@ -181,35 +196,41 @@
     def chunk_copy(idx, ss, to):
         return rc(kvbuf.at[idx], kvbuf.at[idx], ss, k_r.at[idx], to)
 
-    counts = [0, 0]
-
-    def send_on(core, dz, dx):
-        copies = hops(core, dz, dx)
-        if not copies:
-            return
-        first = counts[core]
-        counts[core] += len(copies)
-
-        @pl.when(c == core)
-        def _():
-            idx = zpeer(dz) * NX + xpeer(dx)
-            for i, (axis, step) in enumerate(copies):
-                to = dev(zz=zpeer(step)) if axis == "z" else dev(xx=xpeer(step))
-                chunk_copy(idx, k_s.at[first + i], to).start()
-
     def chunk(n):
-        (z0, x0), (z1, x1) = ORDER0[n], ORDER1[n]
-        dz = z0 * oc + z1 * c
-        dx = x0 * oc + x1 * c
-        return zpeer(dz) * NX + xpeer(dx)
+        k, dx = ORDER[n]
+        return zpeer(-k) * NX + xpeer(dx)
+
+    sent = []
+
+    def send_on(n):
+        k, dx = ORDER[n]
+        idx = chunk(n)
+        for axis, step in hops(k, dx):
+            i = len(sent)
+            if axis == "x":
+                sent.append((k, NZ))
+                chunk_copy(idx, k_s.at[i], dev(xx=xpeer(step))).start()
+            else:
+                sent.append((k, NZ - 1))
+
+                @pl.when(z < NZ - 1)
+                def _():
+                    if k == 0:
+                        pl.semaphore_wait(ready.at[1], 1)
+                    chunk_copy(idx, k_s.at[i], dev(zz=zpeer(step))).start()
 
     def arrivals(first, last):
         for n in range(first, last):
-            if n > 0:
+            k, dx = ORDER[n]
+            if n == 0:
+                send_on(n)
+                continue
+
+            @pl.when(z >= k)
+            def _():
                 idx = chunk(n)
                 rc(kvbuf.at[idx], kvbuf.at[idx], k_s.at[0], k_r.at[idx], partner).wait_recv()
-            send_on(0, *ORDER0[n])
-            send_on(1, *ORDER1[n])
+                send_on(n)
 
     arrivals(0, 1)
     local[C_Q0].wait()
@@ -218,11 +239,6 @@
     qst[...] = qv[:, HD:]
     start(rc(qst, qbuf.at[my64, :], p_s.at[1], p_r.at[1], partner))
     qbuf[my64, :] = qv[:, :HD]
-
-    for d in (1, 3, 2):
-        yy = ypeer(d)
-        cols = pl.ds(pl.multiple_of(yy * 512, 512), 512)
-        start(rc(w_ao.at[:, cols], wo.at[yrows, :], w_s.at[d], w_r.at[y], dev(yy=yy)))
 
     local[C_A].wait()
     local[C_B].wait()
@@ -232,7 +248,24 @@
     gst[...] = gated[32:, :]
     gbuf[32:, :] = gated.astype(F32)
     halo_to = ((next_chip // NX) * c + z * oc, lax.rem(next_chip, NX) * c + x * oc, oc, y)
-    start(rc(gst, halo, halo_s, halo_r, halo_to))
+
+    @pl.when(has_next)
+    def _():
+        pl.semaphore_wait(ready.at[0], 1)
+
+    has_halo = (c == 1) | (chip > 0)
+    sends_halo = (c == 0) | (chip < NCHIP - 1)
+
+    @pl.when(sends_halo)
+    def _():
+        rc(gst, halo, halo_s, halo_r, halo_to).start()
+
+    for i, k in enumerate(WRAPS):
+        @pl.when(z + k < NZ)
+        def _():
+            pl.semaphore_wait(ready.at[k], 1)
+            chunk_copy(chip, wrap_s.at[i], dev(zz=zpeer(k))).start()
+
 
     local[C_GA].wait()
     local[C_GC].wait()
@@ -245,11 +278,8 @@
 
     def blocks(first, last):
         chunks = [chunk(n) for n in range(first, last)]
-        needed = chunks[0] <= chip
-        for idx in chunks[1:]:
-            needed = needed | (idx <= chip)
-
-        @pl.when(needed)
+
+        @pl.when(z >= min(ORDER[n][0] for n in range(first, last)))
         def _():
             fronts = []
             for n, idx in enumerate(chunks, first):
@@ -274,14 +304,15 @@
             for idx, stick in zip(chunks, sticks):
                 obuf[idx] = dot(stick, kvbuf[idx, :, HD:])
 
-    arrivals(1, 4)
-    blocks(0, 4)
-    arrivals(4, 8)
-    blocks(4, 8)
-
-    rc(gst, halo, halo_s, halo_r, halo_to).wait_recv()
-    first = (chip * 2 + c) == 0
-    gbuf[0:32, :] = jnp.where(first, 0.0, halo[...].astype(F32))
+    @pl.when(has_halo)
+    def _():
+        rc(gst, halo, halo_s, halo_r, halo_to).wait_recv()
+        gbuf[0:32, :] = halo[...].astype(F32)
+
+    @pl.when(jnp.logical_not(has_halo))
+    def _():
+        gbuf[0:32, :] = jnp.zeros((32, 256), F32)
+
     conv = jnp.broadcast_to(bias[...], (64, 256))
     for i in range(WIDTH):
         conv = conv + taps[i : i + 1, :] * gbuf[2 + i : 66 + i, :]
@@ -294,11 +325,8 @@
         start(rc(stx, srx.at[y], st_s.at[d], st_r.at[y], dev(yy=ypeer(d))))
     convb[...] = conv
 
-    arrivals(8, 12)
-    blocks(8, 12)
-    arrivals(12, 16)
-    blocks(12, 16)
-
+    arrivals(1, 4)
+    blocks(0, 4)
     srx[y] = stx[...]
     for d in (1, 3, 2):
         yy = ypeer(d)
@@ -318,10 +346,21 @@
         yy = ypeer(d)
         start(rc(cst.at[yy], crx.at[y], c_s.at[d], c_r.at[y], dev(yy=yy)))
 
+    for d in (1, 3, 2):
+        yy = ypeer(d)
+        cols = pl.ds(pl.multiple_of(yy * 512, 512), 512)
+        start(rc(w_ao.at[half, cols], wo.at[whalf(y, c), :], w_s.at[d], w_r.at[y], dev(yy=yy)))
+
+    arrivals(4, 8)
+    blocks(4, 8)
+
+    arrivals(8, 12)
+    blocks(8, 12)
+    arrivals(12, 16)
+    blocks(12, 16)
+
     arrivals(16, 20)
     blocks(16, 20)
-    arrivals(20, 24)
-    blocks(20, 24)
 
     csum = cst[y].astype(F32)
     for d in (1, 3, 2):
@@ -330,8 +369,16 @@
         csum = csum + crx[yy].astype(F32)
     gateb[1] = gateb[1] * csum.astype(BF16).astype(F32)
 
+    arrivals(20, 24)
+    blocks(20, 24)
     arrivals(24, 28)
     blocks(24, 28)
+    for d in (1, 3, 2):
+        yy = ypeer(d)
+        got = wo.at[whalf(yy, c), :]
+        rc(got, got, w_s.at[d], w_r.at[yy], dev(yy=yy)).wait_recv()
+        start(rc(got, got, v_s.at[d], v_r.at[yy], partner))
+
     arrivals(28, 32)
     blocks(28, 32)
 
@@ -356,8 +403,8 @@
     local[C_AO].wait()
     for d in (1, 3, 2):
         yy = ypeer(d)
-        rows = pl.ds(pl.multiple_of(yy * 256, 256), 256)
-        rc(w_ao.at[:, ycols], wo.at[rows, :], w_s.at[d], w_r.at[yy], dev(yy=yy)).wait_recv()
+        came = wo.at[whalf(yy, oc), :]
+        rc(came, came, v_s.at[d], v_r.at[yy], partner).wait_recv()
     for d in (0, 1, 3, 2):
         for cc in (c, oc):
             if d == 0 and cc is c:
@@ -384,12 +431,19 @@
 
     for copy in sends:
         copy.wait_send()
-    for i in range(max(SENDS)):
-        ended = rc(kvbuf.at[chip], kvbuf.at[chip], k_s.at[i], k_r.at[chip], partner).wait_send
-        if i < min(SENDS):
-            ended()
-        else:
-            pl.when(c == SENDS.index(max(SENDS)))(ended)
+    for i, (k, end) in enumerate(sent):
+        @pl.when((z >= k) & (z < end))
+        def _():
+            rc(kvbuf.at[chip], kvbuf.at[chip], k_s.at[i], k_r.at[chip], partner).wait_send()
+
+    for i, k in enumerate(WRAPS):
+        @pl.when(z + k < NZ)
+        def _():
+            rc(kvbuf.at[chip], kvbuf.at[chip], wrap_s.at[i], k_r.at[chip], partner).wait_send()
+
+    @pl.when(sends_halo)
+    def _():
+        rc(gst, halo, halo_s, halo_r, halo_to).wait_send()
 
 
 def on_device(
@@ -439,9 +493,9 @@
             dma((12,)),
             dma((4,)), dma((4,)),
             dma((2,)), dma((2,)),
-            dma((max(SENDS),)), dma((NCHIP,)),
+            dma((SENDS,)), dma((3,)), dma((NCHIP,)), pltpu.SemaphoreType.REGULAR((8,)),
             dma, dma,
-            dma((4,)), dma((4,)),
+            dma((4,)), dma((4,)), dma((4,)), dma((4,)),
             dma((4,)), dma((4,)),
             dma((4,)), dma((4,)),
             dma((7,)), dma((8,)),

time: 53.8 us -> 49.7 us (0.924)
  the two profiles are of different devices: /device:TPU:1 before, /device:TPU:224 now
where the time goes in v3:
time: 49.7 us; the launch traced here: 49.5 us
  Pallas kernels  48 us (97%)
  local copies, waits for them, and re-layouts  1.47 us (3%)
    pallas_call x1, Pallas kernels, on_device(): pl.pallas_call(kernel, out_shape=jax.ShapeDtypeStruct((64, 512), BF16), i...  48 us
    unnamed x1, local copies, waits for them, and re-layouts  1.47 us

profile of v3, /device:TPU:224, one launch (start us, length us, event | category | flops | bytes accessed | tf_op | source)
XLA Modules:
  0.0 49.5 jit_solution(65973715645007463)
XLA Ops:
  0.0 48.0 %shard_map.163 = bf16[64,512]{1,0:T(8,128)(2,1)} custom-call(bf16[16,2048]{1,0:T(8,128)(2,1)} %hidden.1, f32[1,2048]{1,0:T(1,128)} %bitcast.5, bf16[2048,256]{1,0:T(8,128)(2,1)} %w_query.1, bf16[2048,256]{1,0:T(8,128)(2,1)} %w_key.1, bf16[2048,256]{1,0:T(8,128)(2,1)} %w_value.1, f32[2]{0:T(128)} %offset.1, bf16[2048,256]{1,0:T(8,128)(2,1)} %w_a.1, ...), custom_call_target="tpu_custom_call" | custom-call | tf_op jit(solution)/shard_map/pallas_call | solution.py:457
  48.0 1.5 %copy.19 = bf16[64,512]{1,0:T(8,128)(2,1)} copy(bf16[64,512]{1,0:T(8,128)(2,1)} %shard_map.163) | data formatting | bytes 131072

commit v4 on v3

--- a/solution.py
+++ b/solution.py
@@ -23,25 +23,9 @@
 NCHIP = NX * NZ
 
 
-ORDER = (
-    (0, 0), (7, 0), (1, 0), (6, 0), (0, 1), (0, 3), (2, 0), (5, 0),
-    (7, 1), (7, 3), (3, 0), (1, 1), (1, 3), (6, 1), (6, 3), (4, 0),
-    (2, 1), (0, 2), (5, 1), (2, 3), (7, 2), (5, 3), (3, 1), (3, 3),
-    (6, 2), (1, 2), (4, 1), (4, 3), (5, 2), (2, 2), (3, 2), (4, 2),
-)
-UP = 4
+STEPS = (1, 2)
 WRAPS = (7, 6, 5)
-
-
-def hops(k, dx):
-    if dx == 0:
-        return [("x", 1), ("x", 3)] + [("z", 1)] * (k < UP)
-    if dx == 3:
-        return [("x", 1)] if k % 2 == 0 else []
-    return [("x", 3)] if dx == 1 and k % 2 == 1 else []
-
-
-SENDS = sum(len(hops(*t)) for t in ORDER)
+GREETED = STEPS + WRAPS
 
 
 def dot(a, b):
@@ -56,17 +40,17 @@
     return jax.nn.sigmoid(v)
 
 
-(C_K0, C_V0, C_K1, C_V1, C_Q0, C_Q1, C_A, C_B, C_GA, C_GC, C_CO, C_AO) = range(12)
+(C_K0, C_K1, C_V0, C_V1, C_Q0, C_Q1, C_A, C_B, C_GA, C_GC, C_CO, C_AO) = range(12)
 
 
 def kernel(
-    hidden, pre_gain, w_query, w_key, w_value, offset, w_a, w_b, w_ga, w_gc,
-    taps, bias, ngain, nshift, w_ao, w_co, post_gain,
+    hidden_hbm, pre_gain_hbm, w_query, w_key, w_value, offset, w_a, w_b, w_ga, w_gc,
+    taps_hbm, bias_hbm, ngain_hbm, nshift_hbm, w_ao, w_co, post_gain_hbm,
     out,
-    hbuf, wkv_own, wkv_oth, wq, wa, wb, wga, wgc, wco, wo,
-    kvbuf, kvst, qbuf, qst, obuf, tbuf, tri,
+    hidden, pre_gain, taps, bias, ngain, nshift, post_gain, hbuf, wk, wv, wq, wa, wb, wga, wgc, wco, wo,
+    kbuf, vbuf, kst, vst, qbuf, qst, obuf, tbl, tblr, wbuf, ps, pr, tri,
     gst, halo, gbuf, cst, crx, stx, srx, convb, gateb, att, abuf, ssx, ssr,
-    lsem, h_s, h_r, p_s, p_r, k_s, wrap_s, k_r, ready, halo_s, halo_r,
+    lsem, ssem, h_s, h_r, p_s, p_r, z_s, z_r, q_s, q_r, t_s, t_r, o_s, o_r, ready, halo_s, halo_r,
     w_s, w_r, v_s, v_r, st_s, st_r, c_s, c_r, a_s, a_r, ss_s, ss_r,
 ):
     z = lax.axis_index("z")
@@ -110,10 +94,10 @@
     ycols = pl.ds(pl.multiple_of(y * 512, 512), 512)
     yrows = pl.ds(pl.multiple_of(y * 256, 256), 256)
     local = {
-        C_K1: (w_key.at[:, oth_cols], wkv_oth.at[:, lo]),
-        C_V1: (w_value.at[:, oth_cols], wkv_oth.at[:, hi]),
-        C_K0: (w_key.at[:, own_cols], wkv_own.at[:, lo]),
-        C_V0: (w_value.at[:, own_cols], wkv_own.at[:, hi]),
+        C_K1: (w_key.at[:, oth_cols], wk.at[:, lo]),
+        C_K0: (w_key.at[:, own_cols], wk.at[:, hi]),
+        C_V1: (w_value.at[:, oth_cols], wv.at[:, lo]),
+        C_V0: (w_value.at[:, own_cols], wv.at[:, hi]),
         C_Q1: (w_query.at[:, oth_cols], wq.at[:, hi]),
         C_Q0: (w_query.at[:, own_cols], wq.at[:, lo]),
         C_A: (w_a, wa),
@@ -124,9 +108,6 @@
         C_AO: (w_ao.at[:, ycols], wo.at[yrows, :]),
     }
     local = {k: pltpu.make_async_copy(s, d, lsem.at[k]) for k, (s, d) in local.items()}
-    for copy in local.values():
-        copy.start()
-
     barrier = pltpu.get_barrier_semaphore()
     next_chip = lax.rem(chip + 1, NCHIP)
     prev_chip = lax.rem(chip + NCHIP - 1, NCHIP)
@@ -134,11 +115,11 @@
     pz, px = pair_chip // NX, lax.rem(pair_chip, NX)
     greet = [dev(yy=ypeer(d)) for d in (1, 2, 3)]
     greet += [dev(cc=oc, yy=ypeer(d)) for d in (0, 1, 2, 3)]
-    greet += [dev(xx=xpeer(d)) for d in (1, 3)]
+    greet += [dev(xx=xpeer(d), cc=cc) for d in (1, 2, 3) for cc in (c, oc)]
     for peer in greet:
         pl.semaphore_signal(barrier, inc=1, device_id=peer, device_id_type=MESH)
     greeted = len(greet)
-    for k in (1,) + WRAPS:
+    for k in GREETED:
         @pl.when(z + k < NZ)
         def _():
             pl.semaphore_signal(barrier, inc=1, device_id=dev(zz=zpeer(k)), device_id_type=MESH)
@@ -154,17 +135,35 @@
 
     greeted = greeted + jnp.where(has_prev, 1, 0)
 
+    first_in = [(hidden_hbm, hidden), (pre_gain_hbm, pre_gain)]
+    later_in = [
+        (taps_hbm, taps), (bias_hbm, bias), (ngain_hbm, ngain), (nshift_hbm, nshift), (post_gain_hbm, post_gain)
+    ]
+    small = [
+        pltpu.make_async_copy(a, b, ssem.at[i]) for i, (a, b) in enumerate(first_in + later_in)
+    ]
+    for copy in small[:2]:
+        copy.start()
+    for copy in local.values():
+        copy.start()
+    for copy in small[2:]:
+        copy.start()
+
+    r2 = lax.broadcasted_iota(jnp.int32, (2 * HD, HD), 0) % HD
+    c2 = lax.broadcasted_iota(jnp.int32, (2 * HD, HD), 1)
+    tri[...] = jnp.where(r2 > c2, 1.0, 0.0).astype(BF16)
+    obuf[...] = jnp.zeros(obuf.shape, F32)
+    tbl[...] = jnp.zeros(tbl.shape, F32)
+    for copy in small[:2]:
+        copy.wait()
+
     hv = hidden[...].astype(F32)
     inv = lax.rsqrt(jnp.mean(hv * hv, axis=1, keepdims=True) + EPS)
     my16 = pl.ds(pl.multiple_of(y * 16, 16), 16)
     hbuf[my16, :] = (hv * inv * pre_gain[...]).astype(BF16)
 
-    r2 = lax.broadcasted_iota(jnp.int32, (2 * HD, 2 * HD), 0) % HD
-    c2 = lax.broadcasted_iota(jnp.int32, (2 * HD, 2 * HD), 1)
-    tri[...] = jnp.where((r2 > c2) | (c2 >= HD), 1.0, 0.0).astype(BF16)
-
     pl.semaphore_wait(barrier, greeted)
-    for k in (1,) + WRAPS:
+    for k in GREETED:
         @pl.when(z >= k)
         def _():
             pl.semaphore_signal(ready.at[k], inc=1, device_id=dev(zz=zpeer(-k)), device_id_type=MESH)
@@ -184,61 +183,42 @@
     my64 = pl.ds(pl.multiple_of(c * 64, 64), 64)
     oth64 = pl.ds(pl.multiple_of(oc * 64, 64), 64)
     partner = dev(cc=oc)
-    local[C_K1].wait()
-    local[C_V1].wait()
-    kvst[...] = dot(hbuf[...], wkv_oth[...]).astype(BF16)
-    start(rc(kvst, kvbuf.at[chip, my64, :], p_s.at[0], p_r.at[0], partner))
-    local[C_K0].wait()
-    local[C_V0].wait()
-    kvbuf[chip, my64, :] = dot(hbuf[...], wkv_own[...]).astype(BF16)
-    rc(kvst, kvbuf.at[chip, oth64, :], p_s.at[0], p_r.at[0], partner).wait_recv()
-
-    def chunk_copy(idx, ss, to):
-        return rc(kvbuf.at[idx], kvbuf.at[idx], ss, k_r.at[idx], to)
-
-    def chunk(n):
-        k, dx = ORDER[n]
-        return zpeer(-k) * NX + xpeer(dx)
-
-    sent = []
-
-    def send_on(n):
-        k, dx = ORDER[n]
-        idx = chunk(n)
-        for axis, step in hops(k, dx):
-            i = len(sent)
-            if axis == "x":
-                sent.append((k, NZ))
-                chunk_copy(idx, k_s.at[i], dev(xx=xpeer(step))).start()
-            else:
-                sent.append((k, NZ - 1))
-
-                @pl.when(z < NZ - 1)
-                def _():
-                    if k == 0:
-                        pl.semaphore_wait(ready.at[1], 1)
-                    chunk_copy(idx, k_s.at[i], dev(zz=zpeer(step))).start()
-
-    def arrivals(first, last):
-        for n in range(first, last):
-            k, dx = ORDER[n]
-            if n == 0:
-                send_on(n)
-                continue
-
-            @pl.when(z >= k)
+    tables = (kbuf, vbuf)
+    for h, (w, st, copies) in enumerate(((wk, kst, (C_K1, C_K0)), (wv, vst, (C_V1, C_V0)))):
+        for name in copies:
+            local[name].wait()
+        both = dot(hbuf[...], w[...]).astype(BF16)
+        st[...] = both[:, :HD]
+        start(rc(st, tables[h].at[z, my64, :], p_s.at[h], p_r.at[h], partner))
+        tables[h][z, my64, :] = both[:, HD:]
+
+    def z_copy(h, row, i, step):
+        t = tables[h].at[row]
+        return rc(t, t, z_s.at[i], z_r.at[h * NZ + row], dev(zz=zpeer(step)))
+
+    for h in (0, 1):
+        rc(kst, tables[h].at[z, oth64, :], p_s.at[h], p_r.at[h], partner).wait_recv()
+        for i, step in enumerate(STEPS):
+            @pl.when(z < NZ - step)
             def _():
-                idx = chunk(n)
-                rc(kvbuf.at[idx], kvbuf.at[idx], k_s.at[0], k_r.at[idx], partner).wait_recv()
-                send_on(n)
-
-    arrivals(0, 1)
+                if h == 0:
+                    pl.semaphore_wait(ready.at[step], 1)
+                z_copy(h, z, h * 2 + i, step).start()
+
     local[C_Q0].wait()
     local[C_Q1].wait()
     qv = dot(hbuf[...], wq[...]).astype(BF16)
     qst[...] = qv[:, HD:]
-    start(rc(qst, qbuf.at[my64, :], p_s.at[1], p_r.at[1], partner))
-    qbuf[my64, :] = qv[:, :HD]
+
+    def qrows(xx, cc):
+        return pl.ds(pl.multiple_of(xx * HD + cc * 64, 64), 64)
+
+    mine = qbuf.at[qrows(x, c), :]
+    qbuf[qrows(x, c), :] = qv[:, :HD]
+    for d in range(NX):
+        start(rc(qst, mine, q_s.at[d], q_r.at[x * 2 + c], dev(xx=xpeer(d), cc=oc)))
+        if d > 0:
+            start(rc(mine, mine, q_s.at[3 + d], q_r.at[x * 2 + c], dev(xx=xpeer(d))))
 
     local[C_A].wait()
     local[C_B].wait()
@@ -264,45 +244,64 @@
         @pl.when(z + k < NZ)
         def _():
             pl.semaphore_wait(ready.at[k], 1)
-            chunk_copy(chip, wrap_s.at[i], dev(zz=zpeer(k))).start()
-
+            for h in (0, 1):
+                z_copy(h, z, 8 + h * 3 + i, k).start()
 
     local[C_GA].wait()
     local[C_GC].wait()
     gateb[0] = sigmoid(dot(hbuf[...], wga[...]).astype(BF16).astype(F32))
     gateb[1] = sigmoid(dot(hbuf[...], wgc[...]).astype(BF16).astype(F32))
-    rc(qst, qbuf.at[oth64, :], p_s.at[1], p_r.at[1], partner).wait_recv()
+
+    def arrived(h, k):
+        row = zpeer(-k)
+        z_copy(h, row, 0, 1).wait_recv()
+
+    @pl.when(z >= 2)
+    def _():
+        for h in (0, 1):
+            arrived(h, 2)
+            for i, step in enumerate(STEPS):
+                @pl.when(z < NZ - step)
+                def _():
+                    z_copy(h, zpeer(-2), 4 + h * 2 + i, step).start()
+
 
     off = offset[c]
     scale = 1.0 / math.sqrt(HD)
 
-    def blocks(first, last):
-        chunks = [chunk(n) for n in range(first, last)]
-
-        @pl.when(z >= min(ORDER[n][0] for n in range(first, last)))
+    def blocks(k):
+        @pl.when(z >= k)
         def _():
+            row = zpeer(-k)
+            if k not in (0, 2):
+                arrived(0, k)
             fronts = []
-            for n, idx in enumerate(chunks, first):
-                s = dot_nt(qbuf[...], kvbuf[idx, :, 0:HD]) * scale + off
+            for b in range(NX):
+                s = dot_nt(qbuf[b * HD : (b + 1) * HD, :], kbuf[row]) * scale + off
                 u = jnp.exp(-jnp.abs(s))
                 one = 1.0 + u
                 tail = jnp.log(one) + (u - (one - 1.0))
                 soft = jnp.maximum(s, 0.0) + tail
                 logit = s - soft
-                if n == 0:
-                    rows = lax.broadcasted_iota(jnp.int32, (HD, HD), 0)
-                    causal = lax.broadcasted_iota(jnp.int32, (HD, HD), 1) < rows
-                    soft = jnp.where(causal, soft, 0.0)
-                    logit = jnp.where(causal, logit, -jnp.inf)
+                if k == 0:
+                    rows = lax.broadcasted_iota(jnp.int32, (HD, HD), 0) + b * HD
+                    cols = lax.broadcasted_iota(jnp.int32, (HD, HD), 1) + x * HD
+                    soft = jnp.where(cols < rows, soft, 0.0)
+                    logit = jnp.where(cols < rows, logit, -jnp.inf)
                 top = soft.astype(BF16)
                 rest = (soft - top.astype(F32)).astype(BF16)
                 fronts.append((logit, jnp.concatenate([top, rest], axis=1)))
             sums = [dot(pair, tri[...]) for _, pair in fronts]
-            for idx, t in zip(chunks, sums):
-                tbuf[idx] = t[:, HD:]
-            sticks = [jnp.exp(f[0] - t[:, :HD]).astype(BF16) for f, t in zip(fronts, sums)]
-            for idx, stick in zip(chunks, sticks):
-                obuf[idx] = dot(stick, kvbuf[idx, :, HD:])
+            ones = jnp.ones((NZ, 2 * HD), BF16)
+            here = lax.broadcasted_iota(jnp.int32, (NZ, HD), 0) == row
+            for b, (_, pair) in enumerate(fronts):
+                cols = slice(b * HD, (b + 1) * HD)
+                tbl[:, cols] = jnp.where(here, dot_nt(ones, pair), tbl[:, cols])
+            sticks = [jnp.exp(f[0] - t).astype(BF16) for f, t in zip(fronts, sums)]
+            if k not in (0, 2):
+                arrived(1, k)
+            for b, stick in enumerate(sticks):
+                obuf[row, b] = dot(stick, vbuf[row])
 
     @pl.when(has_halo)
     def _():
@@ -313,6 +312,8 @@
     def _():
         gbuf[0:32, :] = jnp.zeros((32, 256), F32)
 
+    for copy in small[2:]:
+        copy.wait()
     conv = jnp.broadcast_to(bias[...], (64, 256))
     for i in range(WIDTH):
         conv = conv + taps[i : i + 1, :] * gbuf[2 + i : 66 + i, :]
@@ -325,8 +326,25 @@
         start(rc(stx, srx.at[y], st_s.at[d], st_r.at[y], dev(yy=ypeer(d))))
     convb[...] = conv
 
-    arrivals(1, 4)
-    blocks(0, 4)
+    for d in (1, 3, 2):
+        yy = ypeer(d)
+        cols = pl.ds(pl.multiple_of(yy * 512, 512), 512)
+        start(rc(w_ao.at[half, cols], wo.at[whalf(y, c), :], w_s.at[d], w_r.at[y], dev(yy=yy)))
+
+    for d in range(NX):
+        for cc in (c, oc):
+            if d == 0 and cc is c:
+                continue
+            got = qbuf.at[qrows(xpeer(d), cc), :]
+            rc(got, got, q_s.at[0], q_r.at[xpeer(d) * 2 + cc], partner).wait_recv()
+
+    blocks(0)
+    blocks(1)
+    blocks(2)
+    blocks(7)
+    blocks(6)
+    blocks(5)
+
     srx[y] = stx[...]
     for d in (1, 3, 2):
         yy = ypeer(d)
@@ -346,21 +364,43 @@
         yy = ypeer(d)
         start(rc(cst.at[yy], crx.at[y], c_s.at[d], c_r.at[y], dev(yy=yy)))
 
-    for d in (1, 3, 2):
-        yy = ypeer(d)
-        cols = pl.ds(pl.multiple_of(yy * 512, 512), 512)
-        start(rc(w_ao.at[half, cols], wo.at[whalf(y, c), :], w_s.at[d], w_r.at[y], dev(yy=yy)))
-
-    arrivals(4, 8)
-    blocks(4, 8)
-
-    arrivals(8, 12)
-    blocks(8, 12)
-    arrivals(12, 16)
-    blocks(12, 16)
-
-    arrivals(16, 20)
-    blocks(16, 20)
+    blocks(3)
+    blocks(4)
+    for d in (1, 3, 2):
+        start(rc(tbl, tblr.at[x], t_s.at[d], t_r.at[x], dev(xx=xpeer(d))))
+    tblr[x] = tbl[...]
+
+    for d in (1, 3, 2):
+        yy = ypeer(d)
+        got = wo.at[whalf(yy, c), :]
+        rc(got, got, w_s.at[d], w_r.at[yy], dev(yy=yy)).wait_recv()
+        start(rc(got, got, v_s.at[d], v_r.at[yy], partner))
+
+    for d in (1, 3, 2):
+        xx = xpeer(d)
+        rc(tbl, tblr.at[xx], t_s.at[d], t_r.at[xx], dev(xx=xx)).wait_recv()
+
+    totals = [tblr[i] for i in range(NX)]
+    row_sum = totals[0] + totals[1] + totals[2] + totals[3]
+    at = lax.broadcasted_iota(jnp.int32, (NZ, NX * HD), 0)
+    outside = jnp.zeros((NZ, NX * HD), F32)
+    for j in range(1, NZ):
+        outside = outside + jnp.where(at < j, row_sum[j : j + 1, :], 0.0)
+    for i in range(1, NX):
+        outside = outside + jnp.where(x < i, 1.0, 0.0) * totals[i]
+    weight = jnp.exp(-outside)
+    for b in range(NX):
+        wbuf[b] = weight[:, b * HD : (b + 1) * HD]
+    for d in (1, 3, 2, 0):
+        b = xpeer(d)
+        per_row = jnp.concatenate([wbuf[b], jnp.zeros((HD - NZ, HD), F32)], axis=0).T
+        acc = obuf[0, b] * per_row[:, 0:1]
+        for j in range(1, NZ):
+            acc = acc + obuf[j, b] * per_row[:, j : j + 1]
+        if d > 0:
+            ps[d] = acc.astype(BF16)
+            start(rc(ps.at[d], pr.at[x], o_s.at[d], o_r.at[x], dev(xx=b)))
+
 
     csum = cst[y].astype(F32)
     for d in (1, 3, 2):
@@ -369,26 +409,10 @@
         csum = csum + crx[yy].astype(F32)
     gateb[1] = gateb[1] * csum.astype(BF16).astype(F32)
 
-    arrivals(20, 24)
-    blocks(20, 24)
-    arrivals(24, 28)
-    blocks(24, 28)
-    for d in (1, 3, 2):
-        yy = ypeer(d)
-        got = wo.at[whalf(yy, c), :]
-        rc(got, got, w_s.at[d], w_r.at[yy], dev(yy=yy)).wait_recv()
-        start(rc(got, got, v_s.at[d], v_r.at[yy], partner))
-
-    arrivals(28, 32)
-    blocks(28, 32)
-
-    def combine(j, state):
-        acc, carry = state
-        idx = chip - j
-        return (acc + obuf[idx] * jnp.exp(-carry), carry + tbuf[idx])
-
-    zero = jnp.zeros((HD, HD), F32)
-    acc, _ = lax.fori_loop(0, chip + 1, combine, (zero, zero))
+    for d in (1, 3, 2):
+        xx = xpeer(d)
+        rc(ps.at[d], pr.at[xx], o_s.at[d], o_r.at[xx], dev(xx=xx)).wait_recv()
+        acc = acc + pr[xx].astype(F32)
     att[...] = acc.astype(BF16)
 
     head = pl.ds(pl.multiple_of((y * 2 + c) * HD, HD), HD)
@@ -431,15 +455,20 @@
 
     for copy in sends:
         copy.wait_send()
-    for i, (k, end) in enumerate(sent):
-        @pl.when((z >= k) & (z < end))
-        def _():
-            rc(kvbuf.at[chip], kvbuf.at[chip], k_s.at[i], k_r.at[chip], partner).wait_send()
-
-    for i, k in enumerate(WRAPS):
-        @pl.when(z + k < NZ)
-        def _():
-            rc(kvbuf.at[chip], kvbuf.at[chip], wrap_s.at[i], k_r.at[chip], partner).wait_send()
+    for h in (0, 1):
+        for i, step in enumerate(STEPS):
+            @pl.when(z < NZ - step)
+            def _():
+                z_copy(h, z, h * 2 + i, step).wait_send()
+
+            @pl.when((z >= 2) & (z < NZ - step))
+            def _():
+                z_copy(h, zpeer(-2), 4 + h * 2 + i, step).wait_send()
+
+        for i, k in enumerate(WRAPS):
+            @pl.when(z + k < NZ)
+            def _():
+                z_copy(h, z, 8 + h * 3 + i, k).wait_send()
 
     @pl.when(sends_halo)
     def _():
@@ -457,9 +486,16 @@
     return pl.pallas_call(
         kernel,
         out_shape=jax.ShapeDtypeStruct((64, 512), BF16),
-        in_specs=[vm, vm, hb, hb, hb, sm, hb, hb, hb, hb, vm, vm, vm, vm, hb, hb, vm],
+        in_specs=[hb] * 5 + [sm] + [hb] * 11,
         out_specs=vm,
         scratch_shapes=[
+            pltpu.VMEM((16, D), BF16),
+            pltpu.VMEM((1, D), F32),
+            pltpu.VMEM((WIDTH, 256), F32),
+            pltpu.VMEM((1, 256), F32),
+            pltpu.VMEM((1, 256), F32),
+            pltpu.VMEM((1, 256), F32),
+            pltpu.VMEM((1, 512), F32),
             pltpu.VMEM((64, D), BF16),
             pltpu.VMEM((D, 256), BF16),
             pltpu.VMEM((D, 256), BF16),
@@ -470,13 +506,19 @@
             pltpu.VMEM((D, 512), BF16),
             pltpu.VMEM((256, D), BF16),
             pltpu.VMEM((1024, 512), BF16),
-            pltpu.VMEM((NCHIP, 128, 256), BF16),
-            pltpu.VMEM((64, 256), BF16),
-            pltpu.VMEM((128, 128), BF16),
+            pltpu.VMEM((NZ, 128, 128), BF16),
+            pltpu.VMEM((NZ, 128, 128), BF16),
             pltpu.VMEM((64, 128), BF16),
-            pltpu.VMEM((NCHIP, 128, 128), F32),
-            pltpu.VMEM((NCHIP, 128, 128), F32),
-            pltpu.VMEM((256, 256), BF16),
+            pltpu.VMEM((64, 128), BF16),
+            pltpu.VMEM((NX * 128, 128), BF16),
+            pltpu.VMEM((64, 128), BF16),
+            pltpu.VMEM((NZ, NX, 128, 128), F32),
+            pltpu.VMEM((NZ, NX * 128), F32),
+            pltpu.VMEM((NX, NZ, NX * 128), F32),
+            pltpu.VMEM((NX, NZ, 128), F32),
+            pltpu.VMEM((NX, 128, 128), BF16),
+            pltpu.VMEM((NX, 128, 128), BF16),
+            pltpu.VMEM((256, 128), BF16),
             pltpu.VMEM((32, 256), BF16),
             pltpu.VMEM((32, 256), BF16),
             pltpu.VMEM((96, 256), F32),
@@ -490,10 +532,14 @@
             pltpu.VMEM((64, 1024), BF16),
             pltpu.VMEM((8, 128), F32),
             pltpu.VMEM((NY, 8, 128), F32),
-            dma((12,)),
+            dma((12,)), dma((7,)),
             dma((4,)), dma((4,)),
             dma((2,)), dma((2,)),
-            dma((SENDS,)), dma((3,)), dma((NCHIP,)), pltpu.SemaphoreType.REGULAR((8,)),
+            dma((14,)), dma((16,)),
+            dma((7,)), dma((8,)),
+            dma((4,)), dma((4,)),
+            dma((4,)), dma((4,)),
+            pltpu.SemaphoreType.REGULAR((8,)),
             dma, dma,
             dma((4,)), dma((4,)), dma((4,)), dma((4,)),
             dma((4,)), dma((4,)),

time: 49.7 us -> 46.5 us (0.936)
  the two profiles are of different devices: /device:TPU:224 before, /device:TPU:192 now
where the time goes in v4:
time: 46.5 us; the launch traced here: 45.8 us
  Pallas kernels  44.3 us (95%)
  local copies, waits for them, and re-layouts  1.47 us (3%)
    pallas_call x1, Pallas kernels, on_device(): pl.pallas_call(kernel, out_shape=jax.ShapeDtypeStruct((64, 512), BF16), i...  44.3 us
    unnamed x1, local copies, waits for them, and re-layouts  1.47 us

profile of v4, /device:TPU:192, one launch (start us, length us, event | category | flops | bytes accessed | tf_op | source)
XLA Modules:
  0.0 45.8 jit_solution(7199616017391039770)
XLA Ops:
  0.0 44.3 %shard_map.163 = bf16[64,512]{1,0:T(8,128)(2,1)} custom-call(bf16[16,2048]{1,0:T(8,128)(2,1)} %hidden_hbm.1, f32[1,2048]{1,0:T(1,128)} %bitcast.5, bf16[2048,256]{1,0:T(8,128)(2,1)} %w_query.1, bf16[2048,256]{1,0:T(8,128)(2,1)} %w_key.1, bf16[2048,256]{1,0:T(8,128)(2,1)} %w_value.1, f32[2]{0:T(128)} %offset.1, bf16[2048,256]{1,0:T(8,128)(2,1)} %w_a.1, ...), custom_call_target="tpu_custom_call" | custom-call | tf_op jit(solution)/shard_map/pallas_call | solution.py:486
  44.3 1.5 %copy.19 = bf16[64,512]{1,0:T(8,128)(2,1)} copy(bf16[64,512]{1,0:T(8,128)(2,1)} %shard_map.163) | data formatting | bytes 131072

commit v5 on v4

--- a/solution.py
+++ b/solution.py
@@ -23,7 +23,7 @@
 NCHIP = NX * NZ
 
 
-STEPS = (1, 2)
+STEPS = (2, 1)
 WRAPS = (7, 6, 5)
 GREETED = STEPS + WRAPS
 
@@ -44,10 +44,10 @@
 
 
 def kernel(
-    hidden_hbm, pre_gain_hbm, w_query, w_key, w_value, offset, w_a, w_b, w_ga, w_gc,
+    hidden_hbm, pre_gain_hbm, w_query, w_key, w_value, offset_hbm, w_a, w_b, w_ga, w_gc,
     taps_hbm, bias_hbm, ngain_hbm, nshift_hbm, w_ao, w_co, post_gain_hbm,
-    out,
-    hidden, pre_gain, taps, bias, ngain, nshift, post_gain, hbuf, wk, wv, wq, wa, wb, wga, wgc, wco, wo,
+    out_hbm,
+    out, offset, hidden, pre_gain, taps, bias, ngain, nshift, post_gain, hbuf, wk, wv, wq, wa, wb, wga, wgc, wco, wo,
     kbuf, vbuf, kst, vst, qbuf, qst, obuf, tbl, tblr, wbuf, ps, pr, tri,
     gst, halo, gbuf, cst, crx, stx, srx, convb, gateb, att, abuf, ssx, ssr,
     lsem, ssem, h_s, h_r, p_s, p_r, z_s, z_r, q_s, q_r, t_s, t_r, o_s, o_r, ready, halo_s, halo_r,
@@ -108,6 +108,17 @@
         C_AO: (w_ao.at[:, ycols], wo.at[yrows, :]),
     }
     local = {k: pltpu.make_async_copy(s, d, lsem.at[k]) for k, (s, d) in local.items()}
+    first_in = [(hidden_hbm, hidden), (pre_gain_hbm, pre_gain)]
+    later_in = [
+        (taps_hbm, taps), (bias_hbm, bias), (ngain_hbm, ngain), (nshift_hbm, nshift), (post_gain_hbm, post_gain),
+        (offset_hbm, offset),
+    ]
+    small = [
+        pltpu.make_async_copy(a, b, ssem.at[i]) for i, (a, b) in enumerate(first_in + later_in)
+    ]
+    for copy in small[:2]:
+        copy.start()
+
     barrier = pltpu.get_barrier_semaphore()
     next_chip = lax.rem(chip + 1, NCHIP)
     prev_chip = lax.rem(chip + NCHIP - 1, NCHIP)
@@ -135,15 +146,27 @@
 
     greeted = greeted + jnp.where(has_prev, 1, 0)
 
-    first_in = [(hidden_hbm, hidden), (pre_gain_hbm, pre_gain)]
-    later_in = [
-        (taps_hbm, taps), (bias_hbm, bias), (ngain_hbm, ngain), (nshift_hbm, nshift), (post_gain_hbm, post_gain)
-    ]
-    small = [
-        pltpu.make_async_copy(a, b, ssem.at[i]) for i, (a, b) in enumerate(first_in + later_in)
-    ]
     for copy in small[:2]:
-        copy.start()
+        copy.wait()
+
+    hv = hidden[...].astype(F32)
+    inv = lax.rsqrt(jnp.mean(hv * hv, axis=1, keepdims=True) + EPS)
+    my16 = pl.ds(pl.multiple_of(y * 16, 16), 16)
+    hbuf[my16, :] = (hv * inv * pre_gain[...]).astype(BF16)
+
+    pl.semaphore_wait(barrier, greeted)
+    for k in GREETED:
+        @pl.when(z >= k)
+        def _():
+            pl.semaphore_signal(ready.at[k], inc=1, device_id=dev(zz=zpeer(-k)), device_id_type=MESH)
+
+    @pl.when(has_prev)
+    def _():
+        pl.semaphore_signal(ready.at[0], inc=1, device_id=next_core, device_id_type=MESH)
+
+
+    for d in (2, 1, 3):
+        start(rc(hbuf.at[my16, :], hbuf.at[my16, :], h_s.at[d], h_r.at[y], dev(yy=ypeer(d))))
     for copy in local.values():
         copy.start()
     for copy in small[2:]:
@@ -154,28 +177,7 @@
     tri[...] = jnp.where(r2 > c2, 1.0, 0.0).astype(BF16)
     obuf[...] = jnp.zeros(obuf.shape, F32)
     tbl[...] = jnp.zeros(tbl.shape, F32)
-    for copy in small[:2]:
-        copy.wait()
-
-    hv = hidden[...].astype(F32)
-    inv = lax.rsqrt(jnp.mean(hv * hv, axis=1, keepdims=True) + EPS)
-    my16 = pl.ds(pl.multiple_of(y * 16, 16), 16)
-    hbuf[my16, :] = (hv * inv * pre_gain[...]).astype(BF16)
-
-    pl.semaphore_wait(barrier, greeted)
-    for k in GREETED:
-        @pl.when(z >= k)
-        def _():
-            pl.semaphore_signal(ready.at[k], inc=1, device_id=dev(zz=zpeer(-k)), device_id_type=MESH)
-
-    @pl.when(has_prev)
-    def _():
-        pl.semaphore_signal(ready.at[0], inc=1, device_id=next_core, device_id_type=MESH)
-
-
-    for d in (1, 3, 2):
-        start(rc(hbuf.at[my16, :], hbuf.at[my16, :], h_s.at[d], h_r.at[y], dev(yy=ypeer(d))))
-    for d in (1, 3, 2):
+    for d in (2, 1, 3):
         yy = ypeer(d)
         rows = pl.ds(pl.multiple_of(yy * 16, 16), 16)
         rc(hbuf.at[rows, :], hbuf.at[rows, :], h_s.at[d], h_r.at[yy], dev(yy=yy)).wait_recv()
@@ -240,6 +242,13 @@
     def _():
         rc(gst, halo, halo_s, halo_r, halo_to).start()
 
+    def send_shard(d):
+        yy = ypeer(d)
+        cols = pl.ds(pl.multiple_of(yy * 512, 512), 512)
+        start(rc(w_ao.at[half, cols], wo.at[whalf(y, c), :], w_s.at[d], w_r.at[y], dev(yy=yy)))
+
+    send_shard(1)
+    send_shard(3)
     for i, k in enumerate(WRAPS):
         @pl.when(z + k < NZ)
         def _():
@@ -247,35 +256,36 @@
             for h in (0, 1):
                 z_copy(h, z, 8 + h * 3 + i, k).start()
 
-    local[C_GA].wait()
-    local[C_GC].wait()
-    gateb[0] = sigmoid(dot(hbuf[...], wga[...]).astype(BF16).astype(F32))
-    gateb[1] = sigmoid(dot(hbuf[...], wgc[...]).astype(BF16).astype(F32))
-
     def arrived(h, k):
         row = zpeer(-k)
         z_copy(h, row, 0, 1).wait_recv()
 
-    @pl.when(z >= 2)
-    def _():
-        for h in (0, 1):
+    def relay(h):
+        @pl.when((z >= 2) & (z < NZ - 1))
+        def _():
             arrived(h, 2)
             for i, step in enumerate(STEPS):
                 @pl.when(z < NZ - step)
                 def _():
                     z_copy(h, zpeer(-2), 4 + h * 2 + i, step).start()
 
-
+    relay(0)
+    small[7].wait()
     off = offset[c]
     scale = 1.0 / math.sqrt(HD)
 
-    def blocks(k):
-        @pl.when(z >= k)
-        def _():
+    def some_blocks(ks):
+        def come(h, k):
+            if k == 2:
+                pl.when(z == NZ - 1)(functools.partial(arrived, h, k))
+            elif k > 0:
+                arrived(h, k)
+
+        for k in ks:
+            come(0, k)
+        fronts = []
+        for k in ks:
             row = zpeer(-k)
-            if k not in (0, 2):
-                arrived(0, k)
-            fronts = []
             for b in range(NX):
                 s = dot_nt(qbuf[b * HD : (b + 1) * HD, :], kbuf[row]) * scale + off
                 u = jnp.exp(-jnp.abs(s))
@@ -290,18 +300,22 @@
                     logit = jnp.where(cols < rows, logit, -jnp.inf)
                 top = soft.astype(BF16)
                 rest = (soft - top.astype(F32)).astype(BF16)
-                fronts.append((logit, jnp.concatenate([top, rest], axis=1)))
-            sums = [dot(pair, tri[...]) for _, pair in fronts]
-            ones = jnp.ones((NZ, 2 * HD), BF16)
+                fronts.append((k, row, b, logit, jnp.concatenate([top, rest], axis=1)))
+        sums = [dot(f[4], tri[...]) for f in fronts]
+        ones = jnp.ones((NZ, 2 * HD), BF16)
+        for k, row, b, _, pair in fronts:
             here = lax.broadcasted_iota(jnp.int32, (NZ, HD), 0) == row
-            for b, (_, pair) in enumerate(fronts):
-                cols = slice(b * HD, (b + 1) * HD)
-                tbl[:, cols] = jnp.where(here, dot_nt(ones, pair), tbl[:, cols])
-            sticks = [jnp.exp(f[0] - t).astype(BF16) for f, t in zip(fronts, sums)]
-            if k not in (0, 2):
-                arrived(1, k)
-            for b, stick in enumerate(sticks):
-                obuf[row, b] = dot(stick, vbuf[row])
+            cols = slice(b * HD, (b + 1) * HD)
+            tbl[:, cols] = jnp.where(here, dot_nt(ones, pair), tbl[:, cols])
+        sticks = [jnp.exp(f[3] - t).astype(BF16) for f, t in zip(fronts, sums)]
+        for k in ks:
+            come(1, k)
+        for (k, row, b, _, _), stick in zip(fronts, sticks):
+            obuf[row, b] = dot(stick, vbuf[row])
+
+    def blocks(low, high):
+        pl.when(z >= high)(functools.partial(some_blocks, (low, high)))
+        pl.when((z >= low) & (z < high))(functools.partial(some_blocks, (low,)))
 
     @pl.when(has_halo)
     def _():
@@ -312,7 +326,7 @@
     def _():
         gbuf[0:32, :] = jnp.zeros((32, 256), F32)
 
-    for copy in small[2:]:
+    for copy in small[2:7]:
         copy.wait()
     conv = jnp.broadcast_to(bias[...], (64, 256))
     for i in range(WIDTH):
@@ -322,15 +336,12 @@
     local_m2 = jnp.sum(dev_local * dev_local, axis=1, keepdims=True)
     lane = lax.broadcasted_iota(jnp.int32, (64, HD), 1)
     stx[...] = jnp.where(lane < 64, local_mean, local_m2)
-    for d in (1, 3, 2):
+    for d in (2, 1, 3):
         start(rc(stx, srx.at[y], st_s.at[d], st_r.at[y], dev(yy=ypeer(d))))
     convb[...] = conv
 
-    for d in (1, 3, 2):
-        yy = ypeer(d)
-        cols = pl.ds(pl.multiple_of(yy * 512, 512), 512)
-        start(rc(w_ao.at[half, cols], wo.at[whalf(y, c), :], w_s.at[d], w_r.at[y], dev(yy=yy)))
-
+    send_shard(2)
+    relay(1)
     for d in range(NX):
         for cc in (c, oc):
             if d == 0 and cc is c:
@@ -338,15 +349,21 @@
             got = qbuf.at[qrows(xpeer(d), cc), :]
             rc(got, got, q_s.at[0], q_r.at[xpeer(d) * 2 + cc], partner).wait_recv()
 
-    blocks(0)
-    blocks(1)
-    blocks(2)
-    blocks(7)
-    blocks(6)
-    blocks(5)
+    blocks(0, 1)
+    blocks(2, 7)
+    blocks(5, 6)
+    blocks(3, 4)
+    for d in (2, 1, 3):
+        start(rc(tbl, tblr.at[x], t_s.at[d], t_r.at[x], dev(xx=xpeer(d))))
+    tblr[x] = tbl[...]
+
+    local[C_GA].wait()
+    local[C_GC].wait()
+    gateb[0] = sigmoid(dot(hbuf[...], wga[...]).astype(BF16).astype(F32))
+    gateb[1] = sigmoid(dot(hbuf[...], wgc[...]).astype(BF16).astype(F32))
 
     srx[y] = stx[...]
-    for d in (1, 3, 2):
+    for d in (2, 1, 3):
         yy = ypeer(d)
         rc(stx, srx.at[yy], st_s.at[d], st_r.at[yy], dev(yy=yy)).wait_recv()
     stats = [srx[i] for i in range(NY)]
@@ -360,23 +377,11 @@
     local[C_CO].wait()
     for i in range(NY):
         cst[i] = dot(cn, wco[:, i * 512 : (i + 1) * 512]).astype(BF16)
-    for d in (1, 3, 2):
+    for d in (2, 1, 3):
         yy = ypeer(d)
         start(rc(cst.at[yy], crx.at[y], c_s.at[d], c_r.at[y], dev(yy=yy)))
 
-    blocks(3)
-    blocks(4)
-    for d in (1, 3, 2):
-        start(rc(tbl, tblr.at[x], t_s.at[d], t_r.at[x], dev(xx=xpeer(d))))
-    tblr[x] = tbl[...]
-
-    for d in (1, 3, 2):
-        yy = ypeer(d)
-        got = wo.at[whalf(yy, c), :]
-        rc(got, got, w_s.at[d], w_r.at[yy], dev(yy=yy)).wait_recv()
-        start(rc(got, got, v_s.at[d], v_r.at[yy], partner))
-
-    for d in (1, 3, 2):
+    for d in (2, 1, 3):
         xx = xpeer(d)
         rc(tbl, tblr.at[xx], t_s.at[d], t_r.at[xx], dev(xx=xx)).wait_recv()
 
@@ -389,11 +394,12 @@
     for i in range(1, NX):
         outside = outside + jnp.where(x < i, 1.0, 0.0) * totals[i]
     weight = jnp.exp(-outside)
+    per_row = jnp.concatenate([weight, jnp.zeros((HD - NZ, NX * HD), F32)], axis=0).T
     for b in range(NX):
-        wbuf[b] = weight[:, b * HD : (b + 1) * HD]
-    for d in (1, 3, 2, 0):
+        wbuf[b] = per_row[b * HD : (b + 1) * HD, :]
+    for d in (2, 1, 3, 0):
         b = xpeer(d)
-        per_row = jnp.concatenate([wbuf[b], jnp.zeros((HD - NZ, HD), F32)], axis=0).T
+        per_row = wbuf[b]
         acc = obuf[0, b] * per_row[:, 0:1]
         for j in range(1, NZ):
             acc = acc + obuf[j, b] * per_row[:, j : j + 1]
@@ -401,15 +407,21 @@
             ps[d] = acc.astype(BF16)
             start(rc(ps.at[d], pr.at[x], o_s.at[d], o_r.at[x], dev(xx=b)))
 
+    for d in (2, 1, 3):
+        yy = ypeer(d)
+        got = wo.at[whalf(yy, c), :]
+        rc(got, got, w_s.at[d], w_r.at[yy], dev(yy=yy)).wait_recv()
+        start(rc(got, got, v_s.at[d], v_r.at[yy], partner))
+
 
     csum = cst[y].astype(F32)
-    for d in (1, 3, 2):
+    for d in (2, 1, 3):
         yy = ypeer(d)
         rc(cst.at[yy], crx.at[yy], c_s.at[d], c_r.at[yy], dev(yy=yy)).wait_recv()
         csum = csum + crx[yy].astype(F32)
     gateb[1] = gateb[1] * csum.astype(BF16).astype(F32)
 
-    for d in (1, 3, 2):
+    for d in (2, 1, 3):
         xx = xpeer(d)
         rc(ps.at[d], pr.at[xx], o_s.at[d], o_r.at[xx], dev(xx=xx)).wait_recv()
         acc = acc + pr[xx].astype(F32)
@@ -417,7 +429,7 @@
 
     head = pl.ds(pl.multiple_of((y * 2 + c) * HD, HD), HD)
     n = 0
-    for d in (0, 1, 3, 2):
+    for d in (2, 1, 3, 0):
         for cc, rows in ((c, my64), (oc, oth64)):
             if d == 0 and cc is c:
                 continue
@@ -425,11 +437,11 @@
             n += 1
     abuf[:, head] = att[my64, :]
     local[C_AO].wait()
-    for d in (1, 3, 2):
+    for d in (2, 1, 3):
         yy = ypeer(d)
         came = wo.at[whalf(yy, oc), :]
         rc(came, came, v_s.at[d], v_r.at[yy], partner).wait_recv()
-    for d in (0, 1, 3, 2):
+    for d in (2, 1, 3, 0):
         for cc in (c, oc):
             if d == 0 and cc is c:
                 continue
@@ -443,16 +455,18 @@
     part = sq[:, 0:128] + sq[:, 128:256] + sq[:, 256:384] + sq[:, 384:512]
     part = jnp.concatenate([part, jnp.zeros((64, HD), F32)], axis=0).T
     ssx[...] = jnp.sum(part.reshape(16, 8, HD), axis=0)
-    for d in (1, 3, 2):
+    for d in (2, 1, 3):
         start(rc(ssx, ssr.at[y], ss_s.at[d], ss_r.at[y], dev(yy=ypeer(d))))
     total = ssx[...]
-    for d in (1, 3, 2):
+    for d in (2, 1, 3):
         yy = ypeer(d)
         rc(ssx, ssr.at[yy], ss_s.at[d], ss_r.at[yy], dev(yy=yy)).wait_recv()
         total = total + ssr[yy]
     total = jnp.broadcast_to(jnp.sum(total, axis=0, keepdims=True), (HD, HD)).T[:64, 0:1]
     out[...] = (merged * lax.rsqrt(total / D + EPS) * post_gain[...]).astype(BF16)
 
+    written = pltpu.make_async_copy(out, out_hbm, ssem.at[8])
+    written.start()
     for copy in sends:
         copy.wait_send()
     for h in (0, 1):
@@ -474,21 +488,23 @@
     def _():
         rc(gst, halo, halo_s, halo_r, halo_to).wait_send()
 
+    written.wait()
+
 
 def on_device(
     hidden_in, pre_gain, w_query, w_key, w_value, stick_offset, w_glu_a, w_glu_b, w_gate_attn,
     w_gate_conv, conv_taps, conv_bias, norm_gain, norm_shift, w_attn_out, w_conv_out, post_gain,
 ):
-    vm = pl.BlockSpec(memory_space=pltpu.VMEM)
     hb = pl.BlockSpec(memory_space=pl.ANY)
-    sm = pl.BlockSpec(memory_space=pltpu.SMEM)
     dma = pltpu.SemaphoreType.DMA
     return pl.pallas_call(
         kernel,
         out_shape=jax.ShapeDtypeStruct((64, 512), BF16),
-        in_specs=[hb] * 5 + [sm] + [hb] * 11,
-        out_specs=vm,
+        in_specs=[hb] * 17,
+        out_specs=hb,
         scratch_shapes=[
+            pltpu.VMEM((64, 512), BF16),
+            pltpu.SMEM((2,), F32),
             pltpu.VMEM((16, D), BF16),
             pltpu.VMEM((1, D), F32),
             pltpu.VMEM((WIDTH, 256), F32),
@@ -515,7 +531,7 @@
             pltpu.VMEM((NZ, NX, 128, 128), F32),
             pltpu.VMEM((NZ, NX * 128), F32),
             pltpu.VMEM((NX, NZ, NX * 128), F32),
-            pltpu.VMEM((NX, NZ, 128), F32),
+            pltpu.VMEM((NX, 128, 128), F32),
             pltpu.VMEM((NX, 128, 128), BF16),
             pltpu.VMEM((NX, 128, 128), BF16),
             pltpu.VMEM((256, 128), BF16),
@@ -532,7 +548,7 @@
             pltpu.VMEM((64, 1024), BF16),
             pltpu.VMEM((8, 128), F32),
             pltpu.VMEM((NY, 8, 128), F32),
-            dma((12,)), dma((7,)),
+            dma((12,)), dma((9,)),
             dma((4,)), dma((4,)),
             dma((2,)), dma((2,)),
             dma((14,)), dma((16,)),

time: 46.5 us -> 42.2 us (0.908); the launches traced: 45.8 us -> 42.1 us
  Pallas kernels: 44.3 us -> 40.6 us
    pallas_call x1, Pallas kernels: 44.3 us -> 40.6 us  [on_device(): pl.pallas_call(kernel, out_shape=jax.ShapeDtypeStruct((64, 512), BF16), i...]
where the time goes in v5:
time: 42.2 us; the launch traced here: 42.1 us
  Pallas kernels  40.6 us (96%)
  local copies, waits for them, and re-layouts  1.47 us (3%)
    pallas_call x1, Pallas kernels, on_device(): pl.pallas_call(kernel, out_shape=jax.ShapeDtypeStruct((64, 512), BF16), i...  40.6 us
    unnamed x1, local copies, waits for them, and re-layouts  1.47 us

profile of v5, /device:TPU:192, one launch (start us, length us, event | category | flops | bytes accessed | tf_op | source)
XLA Modules:
  0.0 42.1 jit_solution(15453559595131145988)
XLA Ops:
  0.0 40.6 %shard_map.163 = bf16[64,512]{1,0:T(8,128)(2,1)} custom-call(bf16[16,2048]{1,0:T(8,128)(2,1)} %hidden_hbm.1, f32[1,2048]{1,0:T(1,128)} %bitcast.5, bf16[2048,256]{1,0:T(8,128)(2,1)} %w_query.1, bf16[2048,256]{1,0:T(8,128)(2,1)} %w_key.1, bf16[2048,256]{1,0:T(8,128)(2,1)} %w_value.1, f32[2]{0:T(128)} %offset_hbm.1, bf16[2048,256]{1,0:T(8,128)(2,1)} %w_a.1, ...), custom_call_target="tpu_custom_call" | custom-call | tf_op jit(solution)/shard_map/pallas_call | solution.py:500
  40.6 1.5 %copy.19 = bf16[64,512]{1,0:T(8,128)(2,1)} copy(bf16[64,512]{1,0:T(8,128)(2,1)} %shard_map.163) | data formatting | bytes 131072

commit v6 on v5

--- a/solution.py
+++ b/solution.py
@@ -46,8 +46,8 @@
 def kernel(
     hidden_hbm, pre_gain_hbm, w_query, w_key, w_value, offset_hbm, w_a, w_b, w_ga, w_gc,
     taps_hbm, bias_hbm, ngain_hbm, nshift_hbm, w_ao, w_co, post_gain_hbm,
-    out_hbm,
-    out, offset, hidden, pre_gain, taps, bias, ngain, nshift, post_gain, hbuf, wk, wv, wq, wa, wb, wga, wgc, wco, wo,
+    out,
+    offset, hidden, pre_gain, taps, bias, ngain, nshift, post_gain, hbuf, wk, wv, wq, wa, wb, wga, wgc, wco, wo,
     kbuf, vbuf, kst, vst, qbuf, qst, obuf, tbl, tblr, wbuf, ps, pr, tri,
     gst, halo, gbuf, cst, crx, stx, srx, convb, gateb, att, abuf, ssx, ssr,
     lsem, ssem, h_s, h_r, p_s, p_r, z_s, z_r, q_s, q_r, t_s, t_r, o_s, o_r, ready, halo_s, halo_r,
@@ -133,9 +133,10 @@
     for k in GREETED:
         @pl.when(z + k < NZ)
         def _():
-            pl.semaphore_signal(barrier, inc=1, device_id=dev(zz=zpeer(k)), device_id_type=MESH)
-
-        greeted = greeted + jnp.where(z >= k, 1, 0)
+            for cc in (c, oc) if k in STEPS else (c,):
+                pl.semaphore_signal(barrier, inc=1, device_id=dev(zz=zpeer(k), cc=cc), device_id_type=MESH)
+
+        greeted = greeted + jnp.where(z >= k, 2 if k in STEPS else 1, 0)
     next_core = (pz, px, oc, y)
     has_next = (c == 1) & (chip < NCHIP - 1)
     has_prev = (c == 0) & (chip > 0)
@@ -158,7 +159,8 @@
     for k in GREETED:
         @pl.when(z >= k)
         def _():
-            pl.semaphore_signal(ready.at[k], inc=1, device_id=dev(zz=zpeer(-k)), device_id_type=MESH)
+            for cc in (c, oc) if k in STEPS else (c,):
+                pl.semaphore_signal(ready.at[k], inc=1, device_id=dev(zz=zpeer(-k), cc=cc), device_id_type=MESH)
 
     @pl.when(has_prev)
     def _():
@@ -198,14 +200,15 @@
         t = tables[h].at[row]
         return rc(t, t, z_s.at[i], z_r.at[h * NZ + row], dev(zz=zpeer(step)))
 
-    for h in (0, 1):
-        rc(kst, tables[h].at[z, oth64, :], p_s.at[h], p_r.at[h], partner).wait_recv()
-        for i, step in enumerate(STEPS):
-            @pl.when(z < NZ - step)
-            def _():
-                if h == 0:
-                    pl.semaphore_wait(ready.at[step], 1)
-                z_copy(h, z, h * 2 + i, step).start()
+    for i, step in enumerate(STEPS):
+        @pl.when(z < NZ - step)
+        def _():
+            pl.semaphore_wait(ready.at[step], 2)
+            for h, st in enumerate((kst, vst)):
+                half_own = tables[h].at[z, my64, :]
+                there = z_r.at[h * NZ + z]
+                rc(half_own, half_own, z_s.at[i], there, dev(zz=zpeer(step))).start()
+                rc(st, half_own, z_s.at[i], there, dev(zz=zpeer(step), cc=oc)).start()
 
     local[C_Q0].wait()
     local[C_Q1].wait()
@@ -249,12 +252,15 @@
 
     send_shard(1)
     send_shard(3)
+    for h in (0, 1):
+        rc(kst, tables[h].at[z, oth64, :], p_s.at[h], p_r.at[h], partner).wait_recv()
+
     for i, k in enumerate(WRAPS):
         @pl.when(z + k < NZ)
         def _():
             pl.semaphore_wait(ready.at[k], 1)
             for h in (0, 1):
-                z_copy(h, z, 8 + h * 3 + i, k).start()
+                z_copy(h, z, 4 + i, k).start()
 
     def arrived(h, k):
         row = zpeer(-k)
@@ -267,7 +273,7 @@
             for i, step in enumerate(STEPS):
                 @pl.when(z < NZ - step)
                 def _():
-                    z_copy(h, zpeer(-2), 4 + h * 2 + i, step).start()
+                    z_copy(h, zpeer(-2), 2 + i, step).start()
 
     relay(0)
     small[7].wait()
@@ -413,14 +419,6 @@
         rc(got, got, w_s.at[d], w_r.at[yy], dev(yy=yy)).wait_recv()
         start(rc(got, got, v_s.at[d], v_r.at[yy], partner))
 
-
-    csum = cst[y].astype(F32)
-    for d in (2, 1, 3):
-        yy = ypeer(d)
-        rc(cst.at[yy], crx.at[yy], c_s.at[d], c_r.at[yy], dev(yy=yy)).wait_recv()
-        csum = csum + crx[yy].astype(F32)
-    gateb[1] = gateb[1] * csum.astype(BF16).astype(F32)
-
     for d in (2, 1, 3):
         xx = xpeer(d)
         rc(ps.at[d], pr.at[xx], o_s.at[d], o_r.at[xx], dev(xx=xx)).wait_recv()
@@ -441,6 +439,14 @@
         yy = ypeer(d)
         came = wo.at[whalf(yy, oc), :]
         rc(came, came, v_s.at[d], v_r.at[yy], partner).wait_recv()
+
+    csum = cst[y].astype(F32)
+    for d in (2, 1, 3):
+        yy = ypeer(d)
+        rc(cst.at[yy], crx.at[yy], c_s.at[d], c_r.at[yy], dev(yy=yy)).wait_recv()
+        csum = csum + crx[yy].astype(F32)
+    gateb[1] = gateb[1] * csum.astype(BF16).astype(F32)
+
     for d in (2, 1, 3, 0):
         for cc in (c, oc):
             if d == 0 and cc is c:
@@ -465,45 +471,43 @@
     total = jnp.broadcast_to(jnp.sum(total, axis=0, keepdims=True), (HD, HD)).T[:64, 0:1]
     out[...] = (merged * lax.rsqrt(total / D + EPS) * post_gain[...]).astype(BF16)
 
-    written = pltpu.make_async_copy(out, out_hbm, ssem.at[8])
-    written.start()
     for copy in sends:
         copy.wait_send()
-    for h in (0, 1):
-        for i, step in enumerate(STEPS):
-            @pl.when(z < NZ - step)
-            def _():
-                z_copy(h, z, h * 2 + i, step).wait_send()
-
-            @pl.when((z >= 2) & (z < NZ - step))
-            def _():
-                z_copy(h, zpeer(-2), 4 + h * 2 + i, step).wait_send()
-
-        for i, k in enumerate(WRAPS):
-            @pl.when(z + k < NZ)
-            def _():
-                z_copy(h, z, 8 + h * 3 + i, k).wait_send()
+    def z_sent(i, cond):
+        @pl.when(cond)
+        def _():
+            two = kbuf.at[0:2]
+            rc(two, two, z_s.at[i], z_r.at[0], partner).wait_send()
+
+    for i, step in enumerate(STEPS):
+        z_sent(i, z < NZ - step)
+        z_sent(2 + i, (z >= 2) & (z < NZ - step))
+    for i, k in enumerate(WRAPS):
+        z_sent(4 + i, z + k < NZ)
 
     @pl.when(sends_halo)
     def _():
         rc(gst, halo, halo_s, halo_r, halo_to).wait_send()
-
-    written.wait()
 
 
 def on_device(
     hidden_in, pre_gain, w_query, w_key, w_value, stick_offset, w_glu_a, w_glu_b, w_gate_attn,
     w_gate_conv, conv_taps, conv_bias, norm_gain, norm_shift, w_attn_out, w_conv_out, post_gain,
 ):
+    args = (
+        hidden_in, pre_gain.reshape(1, -1), w_query, w_key, w_value, stick_offset, w_glu_a,
+        w_glu_b, w_gate_attn, w_gate_conv, conv_taps, conv_bias.reshape(1, -1),
+        norm_gain.reshape(1, -1), norm_shift.reshape(1, -1), w_attn_out, w_conv_out,
+        post_gain.reshape(1, -1),
+    )
     hb = pl.BlockSpec(memory_space=pl.ANY)
     dma = pltpu.SemaphoreType.DMA
     return pl.pallas_call(
         kernel,
         out_shape=jax.ShapeDtypeStruct((64, 512), BF16),
         in_specs=[hb] * 17,
-        out_specs=hb,
+        out_specs=pl.BlockSpec(memory_space=pltpu.VMEM),
         scratch_shapes=[
-            pltpu.VMEM((64, 512), BF16),
             pltpu.SMEM((2,), F32),
             pltpu.VMEM((16, D), BF16),
             pltpu.VMEM((1, D), F32),
@@ -548,10 +552,10 @@
             pltpu.VMEM((64, 1024), BF16),
             pltpu.VMEM((8, 128), F32),
             pltpu.VMEM((NY, 8, 128), F32),
-            dma((12,)), dma((9,)),
+            dma((12,)), dma((8,)),
             dma((4,)), dma((4,)),
             dma((2,)), dma((2,)),
-            dma((14,)), dma((16,)),
+            dma((7,)), dma((16,)),
             dma((7,)), dma((8,)),
             dma((4,)), dma((4,)),
             dma((4,)), dma((4,)),
@@ -564,14 +568,9 @@
             dma((4,)), dma((4,)),
         ],
         compiler_params=pltpu.CompilerParams(
-            collective_id=0, has_side_effects=True, vmem_limit_bytes=56 * 1024 * 1024
+            collective_id=0, has_side_effects=True, vmem_limit_bytes=40 * 1024 * 1024
         ),
-    )(
-        hidden_in, pre_gain.reshape(1, -1), w_query, w_key, w_value, stick_offset, w_glu_a,
-        w_glu_b, w_gate_attn, w_gate_conv, conv_taps, conv_bias.reshape(1, -1),
-        norm_gain.reshape(1, -1), norm_shift.reshape(1, -1), w_attn_out, w_conv_out,
-        post_gain.reshape(1, -1),
-    )
+    )(*(pltpu.with_memory_space_constraint(a, pltpu.HBM) for a in args))
 
 
 def solution(mesh):

time: 42.2 us -> 38.9 us (0.922)
  Pallas kernels: 40.6 us -> 38.1 us
  local copies, waits for them, and re-layouts: 1.47 us -> 0.63 us
    pallas_call x1, Pallas kernels: 40.6 us -> 38.1 us  [on_device(): pl.pallas_call(kernel, out_shape=jax.ShapeDtypeStruct((64, 512), BF16), i...]
    unnamed x1, local copies, waits for them, and re-layouts: 1.47 us -> 0.63 us
where the time goes in v6:
time: 38.9 us; the launch traced here: 38.8 us
  Pallas kernels  38.1 us (98%)
  local copies, waits for them, and re-layouts  0.63 us (2%)
    pallas_call x1, Pallas kernels, on_device(): pl.pallas_call(kernel, out_shape=jax.ShapeDtypeStruct((64, 512), BF16), i...  38.1 us

profile of v6, /device:TPU:192, one launch (start us, length us, event | category | flops | bytes accessed | tf_op | source)
XLA Modules:
  0.0 38.8 jit_solution(158355685974091828)
XLA Ops:
  0.0 38.1 %shard_map.163 = bf16[64,512]{1,0:T(8,128)(2,1)S(1)} custom-call(bf16[16,2048]{1,0:T(8,128)(2,1)} %hidden_hbm.1, f32[1,2048]{1,0:T(1,128)} %bitcast.5, bf16[2048,256]{1,0:T(8,128)(2,1)} %w_query.1, bf16[2048,256]{1,0:T(8,128)(2,1)} %w_key.1, bf16[2048,256]{1,0:T(8,128)(2,1)} %w_value.1, f32[2]{0:T(128)} %offset_hbm.1, bf16[2048,256]{1,0:T(8,128)(2,1)} %w_a.1, ...), custom_call_target="tpu_custom_call" | custom-call | tf_op jit(solution)/shard_map/pallas_call | solution.py:505
  38.1 0.6 %copy.19 = bf16[64,512]{1,0:T(8,128)(2,1)} copy(bf16[64,512]{1,0:T(8,128)(2,1)S(1)} %shard_map.163) | data formatting | bytes 131072

commit v7 on v6

--- a/solution.py
+++ b/solution.py
@@ -40,7 +40,8 @@
     return jax.nn.sigmoid(v)
 
 
-(C_K0, C_K1, C_V0, C_V1, C_Q0, C_Q1, C_A, C_B, C_GA, C_GC, C_CO, C_AO) = range(12)
+(C_K0, C_V0, C_Q0, C_A, C_B, C_GA, C_GC, C_CO, C_AO, C_K1, C_V1, C_Q1) = range(12)
+SHARED = {C_K1: C_K0, C_V1: C_V0, C_Q1: C_Q0}
 
 
 def kernel(
@@ -82,11 +83,26 @@
     def whalf(yy, cc):
         return pl.ds(pl.multiple_of(yy * 256 + cc * HD, HD), HD)
 
-    sends = []
-
     def start(copy):
         copy.start()
-        sends.append(copy)
+
+    def came(whole, group):
+        rc(whole, whole, group[0], group[1], dev(cc=oc)).wait_recv()
+
+    def gone(whole, group):
+        rc(whole, whole, group[0], group[1], dev(cc=oc)).wait_send()
+
+    all_h = hbuf.at[0:48, :], (h_s, h_r)
+    all_p = qbuf.at[0:128, :], (p_s, p_r)
+    all_q = qbuf.at[0:448, :], (q_s, q_r)
+    all_t = tblr.at[0:3], (t_s, t_r)
+    all_o = pr.at[0:3], (o_s, o_r)
+    all_w = wo.at[0:384, :], (w_s, w_r)
+    all_v = wo.at[0:384, :], (v_s, v_r)
+    all_st = srx.at[0:3], (st_s, st_r)
+    all_c = crx.at[0:3], (c_s, c_r)
+    all_a = abuf.at[:, 0:896], (a_s, a_r)
+    all_ss = ssr.at[0:3], (ss_s, ss_r)
 
     own_cols = pl.ds(pl.multiple_of(c * HD, HD), HD)
     oth_cols = pl.ds(pl.multiple_of(oc * HD, HD), HD)
@@ -107,7 +123,7 @@
         C_CO: (w_co, wco),
         C_AO: (w_ao.at[:, ycols], wo.at[yrows, :]),
     }
-    local = {k: pltpu.make_async_copy(s, d, lsem.at[k]) for k, (s, d) in local.items()}
+    local = {k: pltpu.make_async_copy(s, d, lsem.at[SHARED.get(k, k)]) for k, (s, d) in local.items()}
     first_in = [(hidden_hbm, hidden), (pre_gain_hbm, pre_gain)]
     later_in = [
         (taps_hbm, taps), (bias_hbm, bias), (ngain_hbm, ngain), (nshift_hbm, nshift), (post_gain_hbm, post_gain),
@@ -168,7 +184,7 @@
 
 
     for d in (2, 1, 3):
-        start(rc(hbuf.at[my16, :], hbuf.at[my16, :], h_s.at[d], h_r.at[y], dev(yy=ypeer(d))))
+        start(rc(hbuf.at[my16, :], hbuf.at[my16, :], h_s, h_r, dev(yy=ypeer(d))))
     for copy in local.values():
         copy.start()
     for copy in small[2:]:
@@ -179,21 +195,25 @@
     tri[...] = jnp.where(r2 > c2, 1.0, 0.0).astype(BF16)
     obuf[...] = jnp.zeros(obuf.shape, F32)
     tbl[...] = jnp.zeros(tbl.shape, F32)
-    for d in (2, 1, 3):
+    came(*all_h)
+
+    def send_shard(d):
         yy = ypeer(d)
-        rows = pl.ds(pl.multiple_of(yy * 16, 16), 16)
-        rc(hbuf.at[rows, :], hbuf.at[rows, :], h_s.at[d], h_r.at[yy], dev(yy=yy)).wait_recv()
+        cols = pl.ds(pl.multiple_of(yy * 512, 512), 512)
+        start(rc(w_ao.at[half, cols], wo.at[whalf(y, c), :], w_s, w_r, dev(yy=yy)))
+
+    send_shard(1)
+    send_shard(3)
 
     my64 = pl.ds(pl.multiple_of(c * 64, 64), 64)
     oth64 = pl.ds(pl.multiple_of(oc * 64, 64), 64)
     partner = dev(cc=oc)
     tables = (kbuf, vbuf)
-    for h, (w, st, copies) in enumerate(((wk, kst, (C_K1, C_K0)), (wv, vst, (C_V1, C_V0)))):
-        for name in copies:
-            local[name].wait()
+    for h, (w, st, name) in enumerate(((wk, kst, C_K0), (wv, vst, C_V0))):
+        pltpu.make_async_copy(w, w, lsem.at[name]).wait()
         both = dot(hbuf[...], w[...]).astype(BF16)
         st[...] = both[:, :HD]
-        start(rc(st, tables[h].at[z, my64, :], p_s.at[h], p_r.at[h], partner))
+        start(rc(st, tables[h].at[z, my64, :], p_s, p_r, partner))
         tables[h][z, my64, :] = both[:, HD:]
 
     def z_copy(h, row, i, step):
@@ -210,8 +230,7 @@
                 rc(half_own, half_own, z_s.at[i], there, dev(zz=zpeer(step))).start()
                 rc(st, half_own, z_s.at[i], there, dev(zz=zpeer(step), cc=oc)).start()
 
-    local[C_Q0].wait()
-    local[C_Q1].wait()
+    pltpu.make_async_copy(wq, wq, lsem.at[C_Q0]).wait()
     qv = dot(hbuf[...], wq[...]).astype(BF16)
     qst[...] = qv[:, HD:]
 
@@ -221,9 +240,9 @@
     mine = qbuf.at[qrows(x, c), :]
     qbuf[qrows(x, c), :] = qv[:, :HD]
     for d in range(NX):
-        start(rc(qst, mine, q_s.at[d], q_r.at[x * 2 + c], dev(xx=xpeer(d), cc=oc)))
+        start(rc(qst, mine, q_s, q_r, dev(xx=xpeer(d), cc=oc)))
         if d > 0:
-            start(rc(mine, mine, q_s.at[3 + d], q_r.at[x * 2 + c], dev(xx=xpeer(d))))
+            start(rc(mine, mine, q_s, q_r, dev(xx=xpeer(d))))
 
     local[C_A].wait()
     local[C_B].wait()
@@ -245,15 +264,7 @@
     def _():
         rc(gst, halo, halo_s, halo_r, halo_to).start()
 
-    def send_shard(d):
-        yy = ypeer(d)
-        cols = pl.ds(pl.multiple_of(yy * 512, 512), 512)
-        start(rc(w_ao.at[half, cols], wo.at[whalf(y, c), :], w_s.at[d], w_r.at[y], dev(yy=yy)))
-
-    send_shard(1)
-    send_shard(3)
-    for h in (0, 1):
-        rc(kst, tables[h].at[z, oth64, :], p_s.at[h], p_r.at[h], partner).wait_recv()
+    came(*all_p)
 
     for i, k in enumerate(WRAPS):
         @pl.when(z + k < NZ)
@@ -343,24 +354,19 @@
     lane = lax.broadcasted_iota(jnp.int32, (64, HD), 1)
     stx[...] = jnp.where(lane < 64, local_mean, local_m2)
     for d in (2, 1, 3):
-        start(rc(stx, srx.at[y], st_s.at[d], st_r.at[y], dev(yy=ypeer(d))))
+        start(rc(stx, srx.at[y], st_s, st_r, dev(yy=ypeer(d))))
     convb[...] = conv
 
     send_shard(2)
     relay(1)
-    for d in range(NX):
-        for cc in (c, oc):
-            if d == 0 and cc is c:
-                continue
-            got = qbuf.at[qrows(xpeer(d), cc), :]
-            rc(got, got, q_s.at[0], q_r.at[xpeer(d) * 2 + cc], partner).wait_recv()
+    came(*all_q)
 
     blocks(0, 1)
     blocks(2, 7)
     blocks(5, 6)
     blocks(3, 4)
     for d in (2, 1, 3):
-        start(rc(tbl, tblr.at[x], t_s.at[d], t_r.at[x], dev(xx=xpeer(d))))
+        start(rc(tbl, tblr.at[x], t_s, t_r, dev(xx=xpeer(d))))
     tblr[x] = tbl[...]
 
     local[C_GA].wait()
@@ -369,9 +375,7 @@
     gateb[1] = sigmoid(dot(hbuf[...], wgc[...]).astype(BF16).astype(F32))
 
     srx[y] = stx[...]
-    for d in (2, 1, 3):
-        yy = ypeer(d)
-        rc(stx, srx.at[yy], st_s.at[d], st_r.at[yy], dev(yy=yy)).wait_recv()
+    came(*all_st)
     stats = [srx[i] for i in range(NY)]
     means = [t[:, 0:1] for t in stats]
     mean = (means[0] + means[1] + means[2] + means[3]) * 0.25
@@ -385,11 +389,9 @@
         cst[i] = dot(cn, wco[:, i * 512 : (i + 1) * 512]).astype(BF16)
     for d in (2, 1, 3):
         yy = ypeer(d)
-        start(rc(cst.at[yy], crx.at[y], c_s.at[d], c_r.at[y], dev(yy=yy)))
-
-    for d in (2, 1, 3):
-        xx = xpeer(d)
-        rc(tbl, tblr.at[xx], t_s.at[d], t_r.at[xx], dev(xx=xx)).wait_recv()
+        start(rc(cst.at[yy], crx.at[y], c_s, c_r, dev(yy=yy)))
+
+    came(*all_t)
 
     totals = [tblr[i] for i in range(NX)]
     row_sum = totals[0] + totals[1] + totals[2] + totals[3]
@@ -411,50 +413,37 @@
             acc = acc + obuf[j, b] * per_row[:, j : j + 1]
         if d > 0:
             ps[d] = acc.astype(BF16)
-            start(rc(ps.at[d], pr.at[x], o_s.at[d], o_r.at[x], dev(xx=b)))
-
-    for d in (2, 1, 3):
-        yy = ypeer(d)
-        got = wo.at[whalf(yy, c), :]
-        rc(got, got, w_s.at[d], w_r.at[yy], dev(yy=yy)).wait_recv()
-        start(rc(got, got, v_s.at[d], v_r.at[yy], partner))
-
+            start(rc(ps.at[d], pr.at[x], o_s, o_r, dev(xx=b)))
+
+    came(*all_w)
+    for d in (2, 1, 3):
+        got = wo.at[whalf(ypeer(d), c), :]
+        start(rc(got, got, v_s, v_r, partner))
+
+    came(*all_o)
     for d in (2, 1, 3):
         xx = xpeer(d)
-        rc(ps.at[d], pr.at[xx], o_s.at[d], o_r.at[xx], dev(xx=xx)).wait_recv()
         acc = acc + pr[xx].astype(F32)
     att[...] = acc.astype(BF16)
 
     head = pl.ds(pl.multiple_of((y * 2 + c) * HD, HD), HD)
-    n = 0
     for d in (2, 1, 3, 0):
         for cc, rows in ((c, my64), (oc, oth64)):
             if d == 0 and cc is c:
                 continue
-            start(rc(att.at[rows, :], abuf.at[:, head], a_s.at[n], a_r.at[y * 2 + c], dev(cc=cc, yy=ypeer(d))))
-            n += 1
+            start(rc(att.at[rows, :], abuf.at[:, head], a_s, a_r, dev(cc=cc, yy=ypeer(d))))
     abuf[:, head] = att[my64, :]
     local[C_AO].wait()
+    came(*all_v)
+
+    csum = cst[y].astype(F32)
+    came(*all_c)
     for d in (2, 1, 3):
         yy = ypeer(d)
-        came = wo.at[whalf(yy, oc), :]
-        rc(came, came, v_s.at[d], v_r.at[yy], partner).wait_recv()
-
-    csum = cst[y].astype(F32)
-    for d in (2, 1, 3):
-        yy = ypeer(d)
-        rc(cst.at[yy], crx.at[yy], c_s.at[d], c_r.at[yy], dev(yy=yy)).wait_recv()
         csum = csum + crx[yy].astype(F32)
     gateb[1] = gateb[1] * csum.astype(BF16).astype(F32)
 
-    for d in (2, 1, 3, 0):
-        for cc in (c, oc):
-            if d == 0 and cc is c:
-                continue
-            yy = ypeer(d)
-            h = yy * 2 + cc
-            cols = pl.ds(pl.multiple_of(h * HD, HD), HD)
-            rc(att.at[my64, :], abuf.at[:, cols], a_s.at[0], a_r.at[h], dev(cc=oc, yy=yy)).wait_recv()
+    came(*all_a)
     branch = dot(abuf[...], wo[...]).astype(BF16).astype(F32)
     merged = gateb[0] * branch + gateb[1]
     sq = merged * merged
@@ -462,17 +451,16 @@
     part = jnp.concatenate([part, jnp.zeros((64, HD), F32)], axis=0).T
     ssx[...] = jnp.sum(part.reshape(16, 8, HD), axis=0)
     for d in (2, 1, 3):
-        start(rc(ssx, ssr.at[y], ss_s.at[d], ss_r.at[y], dev(yy=ypeer(d))))
+        start(rc(ssx, ssr.at[y], ss_s, ss_r, dev(yy=ypeer(d))))
     total = ssx[...]
-    for d in (2, 1, 3):
-        yy = ypeer(d)
-        rc(ssx, ssr.at[yy], ss_s.at[d], ss_r.at[yy], dev(yy=yy)).wait_recv()
-        total = total + ssr[yy]
+    came(*all_ss)
+    for d in (2, 1, 3):
+        total = total + ssr[ypeer(d)]
     total = jnp.broadcast_to(jnp.sum(total, axis=0, keepdims=True), (HD, HD)).T[:64, 0:1]
     out[...] = (merged * lax.rsqrt(total / D + EPS) * post_gain[...]).astype(BF16)
 
-    for copy in sends:
-        copy.wait_send()
+    for group in (all_h, all_p, all_q, all_t, all_o, all_w, all_v, all_st, all_c, all_a, all_ss):
+        gone(*group)
     def z_sent(i, cond):
         @pl.when(cond)
         def _():
@@ -552,20 +540,20 @@
             pltpu.VMEM((64, 1024), BF16),
             pltpu.VMEM((8, 128), F32),
             pltpu.VMEM((NY, 8, 128), F32),
-            dma((12,)), dma((8,)),
-            dma((4,)), dma((4,)),
-            dma((2,)), dma((2,)),
+            dma((9,)), dma((8,)),
+            dma, dma,
+            dma, dma,
             dma((7,)), dma((16,)),
-            dma((7,)), dma((8,)),
-            dma((4,)), dma((4,)),
-            dma((4,)), dma((4,)),
+            dma, dma,
+            dma, dma,
+            dma, dma,
             pltpu.SemaphoreType.REGULAR((8,)),
             dma, dma,
-            dma((4,)), dma((4,)), dma((4,)), dma((4,)),
-            dma((4,)), dma((4,)),
-            dma((4,)), dma((4,)),
-            dma((7,)), dma((8,)),
-            dma((4,)), dma((4,)),
+            dma, dma, dma, dma,
+            dma, dma,
+            dma, dma,
+            dma, dma,
+            dma, dma,
         ],
         compiler_params=pltpu.CompilerParams(
             collective_id=0, has_side_effects=True, vmem_limit_bytes=40 * 1024 * 1024

time: 38.9 us -> 38.1 us (0.979)
  Pallas kernels: 38.1 us -> 37.3 us
    pallas_call x1, Pallas kernels: 38.1 us -> 37.3 us  [on_device(): pl.pallas_call(kernel, out_shape=jax.ShapeDtypeStruct((64, 512), BF16), i...]
where the time goes in v7:
time: 38.1 us; the launch traced here: 38 us
  Pallas kernels  37.3 us (98%)
  local copies, waits for them, and re-layouts  0.63 us (2%)
    pallas_call x1, Pallas kernels, on_device(): pl.pallas_call(kernel, out_shape=jax.ShapeDtypeStruct((64, 512), BF16), i...  37.3 us

profile of v7, /device:TPU:192, one launch (start us, length us, event | category | flops | bytes accessed | tf_op | source)
XLA Modules:
  0.0 38.0 jit_solution(11952904625458920957)
XLA Ops:
  0.0 37.3 %shard_map.163 = bf16[64,512]{1,0:T(8,128)(2,1)S(1)} custom-call(bf16[16,2048]{1,0:T(8,128)(2,1)} %hidden_hbm.1, f32[1,2048]{1,0:T(1,128)} %bitcast.5, bf16[2048,256]{1,0:T(8,128)(2,1)} %w_query.1, bf16[2048,256]{1,0:T(8,128)(2,1)} %w_key.1, bf16[2048,256]{1,0:T(8,128)(2,1)} %w_value.1, f32[2]{0:T(128)} %offset_hbm.1, bf16[2048,256]{1,0:T(8,128)(2,1)} %w_a.1, ...), custom_call_target="tpu_custom_call" | custom-call | tf_op jit(solution)/shard_map/pallas_call | solution.py:493
  37.4 0.6 %copy.19 = bf16[64,512]{1,0:T(8,128)(2,1)} copy(bf16[64,512]{1,0:T(8,128)(2,1)S(1)} %shard_map.163) | data formatting | bytes 131072

commit v8 on v7

--- a/solution.py
+++ b/solution.py
@@ -49,7 +49,7 @@
     taps_hbm, bias_hbm, ngain_hbm, nshift_hbm, w_ao, w_co, post_gain_hbm,
     out,
     offset, hidden, pre_gain, taps, bias, ngain, nshift, post_gain, hbuf, wk, wv, wq, wa, wb, wga, wgc, wco, wo,
-    kbuf, vbuf, kst, vst, qbuf, qst, obuf, tbl, tblr, wbuf, ps, pr, tri,
+    kbuf, vbuf, kst, vst, qbuf, qst, obuf, stk, tbl, tblr, wbuf, own, ps, pr, tri,
     gst, halo, gbuf, cst, crx, stx, srx, convb, gateb, att, abuf, ssx, ssr,
     lsem, ssem, h_s, h_r, p_s, p_r, z_s, z_r, q_s, q_r, t_s, t_r, o_s, o_r, ready, halo_s, halo_r,
     w_s, w_r, v_s, v_r, st_s, st_r, c_s, c_r, a_s, a_r, ss_s, ss_r,
@@ -96,7 +96,7 @@
     all_p = qbuf.at[0:128, :], (p_s, p_r)
     all_q = qbuf.at[0:448, :], (q_s, q_r)
     all_t = tblr.at[0:3], (t_s, t_r)
-    all_o = pr.at[0:3], (o_s, o_r)
+    all_o = [(pr.at[0:3, i * 64 : (i + 1) * 64], (o_s.at[i], o_r.at[i])) for i in (0, 1)]
     all_w = wo.at[0:384, :], (w_s, w_r)
     all_v = wo.at[0:384, :], (v_s, v_r)
     all_st = srx.at[0:3], (st_s, st_r)
@@ -291,13 +291,13 @@
     off = offset[c]
     scale = 1.0 / math.sqrt(HD)
 
+    def come(h, k):
+        if k == 2:
+            pl.when(z == NZ - 1)(functools.partial(arrived, h, k))
+        elif k > 0:
+            arrived(h, k)
+
     def some_blocks(ks):
-        def come(h, k):
-            if k == 2:
-                pl.when(z == NZ - 1)(functools.partial(arrived, h, k))
-            elif k > 0:
-                arrived(h, k)
-
         for k in ks:
             come(0, k)
         fronts = []
@@ -324,11 +324,8 @@
             here = lax.broadcasted_iota(jnp.int32, (NZ, HD), 0) == row
             cols = slice(b * HD, (b + 1) * HD)
             tbl[:, cols] = jnp.where(here, dot_nt(ones, pair), tbl[:, cols])
-        sticks = [jnp.exp(f[3] - t).astype(BF16) for f, t in zip(fronts, sums)]
-        for k in ks:
-            come(1, k)
-        for (k, row, b, _, _), stick in zip(fronts, sticks):
-            obuf[row, b] = dot(stick, vbuf[row])
+        for (k, row, b, logit, _), t in zip(fronts, sums):
+            stk[k, b * HD : (b + 1) * HD, :] = jnp.exp(logit - t).astype(BF16)
 
     def blocks(low, high):
         pl.when(z >= high)(functools.partial(some_blocks, (low, high)))
@@ -368,11 +365,6 @@
     for d in (2, 1, 3):
         start(rc(tbl, tblr.at[x], t_s, t_r, dev(xx=xpeer(d))))
     tblr[x] = tbl[...]
-
-    local[C_GA].wait()
-    local[C_GC].wait()
-    gateb[0] = sigmoid(dot(hbuf[...], wga[...]).astype(BF16).astype(F32))
-    gateb[1] = sigmoid(dot(hbuf[...], wgc[...]).astype(BF16).astype(F32))
 
     srx[y] = stx[...]
     came(*all_st)
@@ -391,6 +383,13 @@
         yy = ypeer(d)
         start(rc(cst.at[yy], crx.at[y], c_s, c_r, dev(yy=yy)))
 
+    for k in (0, 1, 2, 7, 6, 5, 3, 4):
+        @pl.when(z >= k)
+        def _():
+            come(1, k)
+            row = zpeer(-k)
+            obuf[row] = dot(stk[k], vbuf[row])
+
     came(*all_t)
 
     totals = [tblr[i] for i in range(NX)]
@@ -402,37 +401,53 @@
     for i in range(1, NX):
         outside = outside + jnp.where(x < i, 1.0, 0.0) * totals[i]
     weight = jnp.exp(-outside)
-    per_row = jnp.concatenate([weight, jnp.zeros((HD - NZ, NX * HD), F32)], axis=0).T
+    per_row = weight.T
     for b in range(NX):
         wbuf[b] = per_row[b * HD : (b + 1) * HD, :]
     for d in (2, 1, 3, 0):
         b = xpeer(d)
         per_row = wbuf[b]
-        acc = obuf[0, b] * per_row[:, 0:1]
+        rows = pl.ds(pl.multiple_of(b * HD, HD), HD)
+        acc = obuf[0, rows, :] * per_row[:, 0:1]
         for j in range(1, NZ):
-            acc = acc + obuf[j, b] * per_row[:, j : j + 1]
+            acc = acc + obuf[j, rows, :] * per_row[:, j : j + 1]
         if d > 0:
             ps[d] = acc.astype(BF16)
-            start(rc(ps.at[d], pr.at[x], o_s, o_r, dev(xx=b)))
+        else:
+            own[...] = acc
+    halves = [slice(i * 64, (i + 1) * 64) for i in (0, 1)]
+    for i in (0, 1):
+        for d in (2, 1, 3):
+            start(rc(ps.at[d, halves[i]], pr.at[x, halves[i]], o_s.at[i], o_r.at[i], dev(xx=xpeer(d))))
 
     came(*all_w)
     for d in (2, 1, 3):
         got = wo.at[whalf(ypeer(d), c), :]
         start(rc(got, got, v_s, v_r, partner))
 
-    came(*all_o)
-    for d in (2, 1, 3):
-        xx = xpeer(d)
-        acc = acc + pr[xx].astype(F32)
-    att[...] = acc.astype(BF16)
+    local[C_GA].wait()
+    local[C_GC].wait()
+    gateb[0] = sigmoid(dot(hbuf[...], wga[...]).astype(BF16).astype(F32))
+    gateb[1] = sigmoid(dot(hbuf[...], wgc[...]).astype(BF16).astype(F32))
 
     head = pl.ds(pl.multiple_of((y * 2 + c) * HD, HD), HD)
-    for d in (2, 1, 3, 0):
-        for cc, rows in ((c, my64), (oc, oth64)):
-            if d == 0 and cc is c:
-                continue
-            start(rc(att.at[rows, :], abuf.at[:, head], a_s, a_r, dev(cc=cc, yy=ypeer(d))))
-    abuf[:, head] = att[my64, :]
+    for i, rows in enumerate(halves):
+        came(*all_o[i])
+        acc = own[rows, :]
+        for d in (2, 1, 3):
+            acc = acc + pr[xpeer(d), rows, :].astype(F32)
+        att[rows, :] = acc.astype(BF16)
+        for d in (2, 1, 3):
+            start(rc(att.at[rows, :], abuf.at[:, head], a_s, a_r, dev(cc=i, yy=ypeer(d))))
+
+        @pl.when(c == i)
+        def _():
+            abuf[:, head] = att[rows, :]
+
+        @pl.when(c != i)
+        def _():
+            rc(att.at[rows, :], abuf.at[:, head], a_s, a_r, dev(cc=i)).start()
+
     local[C_AO].wait()
     came(*all_v)
 
@@ -459,7 +474,7 @@
     total = jnp.broadcast_to(jnp.sum(total, axis=0, keepdims=True), (HD, HD)).T[:64, 0:1]
     out[...] = (merged * lax.rsqrt(total / D + EPS) * post_gain[...]).astype(BF16)
 
-    for group in (all_h, all_p, all_q, all_t, all_o, all_w, all_v, all_st, all_c, all_a, all_ss):
+    for group in (all_h, all_p, all_q, all_t, *all_o, all_w, all_v, all_st, all_c, all_a, all_ss):
         gone(*group)
     def z_sent(i, cond):
         @pl.when(cond)
@@ -520,10 +535,12 @@
             pltpu.VMEM((64, 128), BF16),
             pltpu.VMEM((NX * 128, 128), BF16),
             pltpu.VMEM((64, 128), BF16),
-            pltpu.VMEM((NZ, NX, 128, 128), F32),
+            pltpu.VMEM((NZ, NX * 128, 128), F32),
+            pltpu.VMEM((NZ, NX * 128, 128), BF16),
             pltpu.VMEM((NZ, NX * 128), F32),
             pltpu.VMEM((NX, NZ, NX * 128), F32),
-            pltpu.VMEM((NX, 128, 128), F32),
+            pltpu.VMEM((NX, 128, NZ), F32),
+            pltpu.VMEM((128, 128), F32),
             pltpu.VMEM((NX, 128, 128), BF16),
             pltpu.VMEM((NX, 128, 128), BF16),
             pltpu.VMEM((256, 128), BF16),
@@ -546,7 +563,7 @@
             dma((7,)), dma((16,)),
             dma, dma,
             dma, dma,
-            dma, dma,
+            dma((2,)), dma((2,)),
             pltpu.SemaphoreType.REGULAR((8,)),
             dma, dma,
             dma, dma, dma, dma,

time: 38.1 us -> 37.3 us (0.979)
  Pallas kernels: 37.3 us -> 36.6 us
    pallas_call x1, Pallas kernels: 37.3 us -> 36.6 us  [on_device(): pl.pallas_call(kernel, out_shape=jax.ShapeDtypeStruct((64, 512), BF16), i...]
where the time goes in v8:
time: 37.3 us; the launch traced here: 37.2 us
  Pallas kernels  36.6 us (98%)
  local copies, waits for them, and re-layouts  0.63 us (2%)
    pallas_call x1, Pallas kernels, on_device(): pl.pallas_call(kernel, out_shape=jax.ShapeDtypeStruct((64, 512), BF16), i...  36.6 us

profile of v8, /device:TPU:192, one launch (start us, length us, event | category | flops | bytes accessed | tf_op | source)
XLA Modules:
  0.0 37.2 jit_solution(14307606545255376976)
XLA Ops:
  0.0 36.6 %shard_map.163 = bf16[64,512]{1,0:T(8,128)(2,1)S(1)} custom-call(bf16[16,2048]{1,0:T(8,128)(2,1)} %hidden_hbm.1, f32[1,2048]{1,0:T(1,128)} %bitcast.5, bf16[2048,256]{1,0:T(8,128)(2,1)} %w_query.1, bf16[2048,256]{1,0:T(8,128)(2,1)} %w_key.1, bf16[2048,256]{1,0:T(8,128)(2,1)} %w_value.1, f32[2]{0:T(128)} %offset_hbm.1, bf16[2048,256]{1,0:T(8,128)(2,1)} %w_a.1, ...), custom_call_target="tpu_custom_call" | custom-call | tf_op jit(solution)/shard_map/pallas_call | solution.py:508
  36.6 0.6 %copy.19 = bf16[64,512]{1,0:T(8,128)(2,1)} copy(bf16[64,512]{1,0:T(8,128)(2,1)S(1)} %shard_map.163) | data formatting | bytes 131072

commit v9 on v8

--- a/solution.py
+++ b/solution.py
@@ -209,26 +209,31 @@
     oth64 = pl.ds(pl.multiple_of(oc * 64, 64), 64)
     partner = dev(cc=oc)
     tables = (kbuf, vbuf)
+
+    def z_own(h, i):
+        step = STEPS[i]
+
+        @pl.when(z < NZ - step)
+        def _():
+            if h == 0:
+                pl.semaphore_wait(ready.at[step], 2)
+            mine, there = tables[h].at[z, my64, :], z_r.at[h * NZ + z]
+            rc(mine, mine, z_s.at[i], there, dev(zz=zpeer(step))).start()
+            rc((kst, vst)[h], mine, z_s.at[i], there, dev(zz=zpeer(step), cc=oc)).start()
+
     for h, (w, st, name) in enumerate(((wk, kst, C_K0), (wv, vst, C_V0))):
         pltpu.make_async_copy(w, w, lsem.at[name]).wait()
         both = dot(hbuf[...], w[...]).astype(BF16)
         st[...] = both[:, :HD]
         start(rc(st, tables[h].at[z, my64, :], p_s, p_r, partner))
         tables[h][z, my64, :] = both[:, HD:]
+        z_own(h, 0)
+        if h == 0:
+            z_own(h, 1)
 
     def z_copy(h, row, i, step):
         t = tables[h].at[row]
         return rc(t, t, z_s.at[i], z_r.at[h * NZ + row], dev(zz=zpeer(step)))
-
-    for i, step in enumerate(STEPS):
-        @pl.when(z < NZ - step)
-        def _():
-            pl.semaphore_wait(ready.at[step], 2)
-            for h, st in enumerate((kst, vst)):
-                half_own = tables[h].at[z, my64, :]
-                there = z_r.at[h * NZ + z]
-                rc(half_own, half_own, z_s.at[i], there, dev(zz=zpeer(step))).start()
-                rc(st, half_own, z_s.at[i], there, dev(zz=zpeer(step), cc=oc)).start()
 
     pltpu.make_async_copy(wq, wq, lsem.at[C_Q0]).wait()
     qv = dot(hbuf[...], wq[...]).astype(BF16)
@@ -287,6 +292,7 @@
                     z_copy(h, zpeer(-2), 2 + i, step).start()
 
     relay(0)
+    z_own(1, 1)
     small[7].wait()
     off = offset[c]
     scale = 1.0 / math.sqrt(HD)
@@ -355,13 +361,21 @@
     convb[...] = conv
 
     send_shard(2)
+    came(*all_q)
+
+    blocks(0, 1)
     relay(1)
-    came(*all_q)
-
-    blocks(0, 1)
     blocks(2, 7)
+    @pl.when(z < NZ - 2)
+    def _():
+        blocks(3, 4)
+
     blocks(5, 6)
-    blocks(3, 4)
+
+    @pl.when(z >= NZ - 2)
+    def _():
+        some_blocks((3, 4))
+
     for d in (2, 1, 3):
         start(rc(tbl, tblr.at[x], t_s, t_r, dev(xx=xpeer(d))))
     tblr[x] = tbl[...]

time: 37.3 us -> 36.5 us (0.979)
  the two profiles are of different devices: /device:TPU:192 before, /device:TPU:162 now
where the time goes in v9:
time: 36.5 us; the launch traced here: 36.4 us
  Pallas kernels  35.7 us (98%)
  local copies, waits for them, and re-layouts  0.63 us (2%)
    pallas_call x1, Pallas kernels, on_device(): pl.pallas_call(kernel, out_shape=jax.ShapeDtypeStruct((64, 512), BF16), i...  35.7 us

profile of v9, /device:TPU:162, one launch (start us, length us, event | category | flops | bytes accessed | tf_op | source)
XLA Modules:
  0.0 36.4 jit_solution(12141258881472477895)
XLA Ops:
  0.0 35.7 %shard_map.163 = bf16[64,512]{1,0:T(8,128)(2,1)S(1)} custom-call(bf16[16,2048]{1,0:T(8,128)(2,1)} %hidden_hbm.1, f32[1,2048]{1,0:T(1,128)} %bitcast.5, bf16[2048,256]{1,0:T(8,128)(2,1)} %w_query.1, bf16[2048,256]{1,0:T(8,128)(2,1)} %w_key.1, bf16[2048,256]{1,0:T(8,128)(2,1)} %w_value.1, f32[2]{0:T(128)} %offset_hbm.1, bf16[2048,256]{1,0:T(8,128)(2,1)} %w_a.1, ...), custom_call_target="tpu_custom_call" | custom-call | tf_op jit(solution)/shard_map/pallas_call | solution.py:522
  35.7 0.6 %copy.19 = bf16[64,512]{1,0:T(8,128)(2,1)} copy(bf16[64,512]{1,0:T(8,128)(2,1)S(1)} %shard_map.163) | data formatting | bytes 131072

commit v10 on v9

--- a/solution.py
+++ b/solution.py
@@ -24,7 +24,7 @@
 
 
 STEPS = (2, 1)
-WRAPS = (7, 6, 5)
+WRAPS = (5, 6, 7)
 GREETED = STEPS + WRAPS
 
 
@@ -210,10 +210,10 @@
     partner = dev(cc=oc)
     tables = (kbuf, vbuf)
 
-    def z_own(h, i):
+    def z_own(h, i, cond=True):
         step = STEPS[i]
 
-        @pl.when(z < NZ - step)
+        @pl.when((z < NZ - step) & cond)
         def _():
             if h == 0:
                 pl.semaphore_wait(ready.at[step], 2)
@@ -221,20 +221,24 @@
             rc(mine, mine, z_s.at[i], there, dev(zz=zpeer(step))).start()
             rc((kst, vst)[h], mine, z_s.at[i], there, dev(zz=zpeer(step), cc=oc)).start()
 
-    for h, (w, st, name) in enumerate(((wk, kst, C_K0), (wv, vst, C_V0))):
+    def z_copy(h, row, i, step):
+        t = tables[h].at[row]
+        return rc(t, t, z_s.at[i], z_r.at[h * NZ + row], dev(zz=zpeer(step)))
+
+    def project(h):
+        w, st, name = ((wk, kst, C_K0), (wv, vst, C_V0))[h]
         pltpu.make_async_copy(w, w, lsem.at[name]).wait()
         both = dot(hbuf[...], w[...]).astype(BF16)
         st[...] = both[:, :HD]
         start(rc(st, tables[h].at[z, my64, :], p_s, p_r, partner))
         tables[h][z, my64, :] = both[:, HD:]
-        z_own(h, 0)
         if h == 0:
+            z_own(h, 0)
             z_own(h, 1)
-
-    def z_copy(h, row, i, step):
-        t = tables[h].at[row]
-        return rc(t, t, z_s.at[i], z_r.at[h * NZ + row], dev(zz=zpeer(step)))
-
+        else:
+            z_own(h, 0, c == 0)
+
+    project(0)
     pltpu.make_async_copy(wq, wq, lsem.at[C_Q0]).wait()
     qv = dot(hbuf[...], wq[...]).astype(BF16)
     qst[...] = qv[:, HD:]
@@ -249,6 +253,7 @@
         if d > 0:
             start(rc(mine, mine, q_s, q_r, dev(xx=xpeer(d))))
 
+    project(1)
     local[C_A].wait()
     local[C_B].wait()
     left = dot(hbuf[...], wa[...]).astype(BF16).astype(F32)
@@ -271,19 +276,22 @@
 
     came(*all_p)
 
-    for i, k in enumerate(WRAPS):
-        @pl.when(z + k < NZ)
-        def _():
-            pl.semaphore_wait(ready.at[k], 1)
-            for h in (0, 1):
+    def wrap(h):
+        for i, k in enumerate(WRAPS):
+            @pl.when(z + k < NZ)
+            def _():
+                if h == 0:
+                    pl.semaphore_wait(ready.at[k], 1)
                 z_copy(h, z, 4 + i, k).start()
+
+    wrap(0)
 
     def arrived(h, k):
         row = zpeer(-k)
         z_copy(h, row, 0, 1).wait_recv()
 
-    def relay(h):
-        @pl.when((z >= 2) & (z < NZ - 1))
+    def relay(h, low=2, high=NZ - 1):
+        @pl.when((z >= low) & (z < high))
         def _():
             arrived(h, 2)
             for i, step in enumerate(STEPS):
@@ -292,6 +300,7 @@
                     z_copy(h, zpeer(-2), 2 + i, step).start()
 
     relay(0)
+    z_own(1, 0, c == 1)
     z_own(1, 1)
     small[7].wait()
     off = offset[c]
@@ -361,25 +370,27 @@
     convb[...] = conv
 
     send_shard(2)
+    wrap(1)
     came(*all_q)
 
     blocks(0, 1)
-    relay(1)
-    blocks(2, 7)
-    @pl.when(z < NZ - 2)
-    def _():
-        blocks(3, 4)
-
-    blocks(5, 6)
-
-    @pl.when(z >= NZ - 2)
-    def _():
-        some_blocks((3, 4))
+    @pl.when((z >= 2) & (z < 5))
+    def _():
+        some_blocks((2,))
+
+    @pl.when(z >= 5)
+    def _():
+        some_blocks((2, 5))
+
+    relay(1, high=5)
+    blocks(6, 7)
+    blocks(3, 4)
 
     for d in (2, 1, 3):
         start(rc(tbl, tblr.at[x], t_s, t_r, dev(xx=xpeer(d))))
     tblr[x] = tbl[...]
 
+    relay(1, low=5)
     srx[y] = stx[...]
     came(*all_st)
     stats = [srx[i] for i in range(NY)]

time: 36.5 us -> 35.8 us (0.981)
  the two profiles are of different devices: /device:TPU:162 before, /device:TPU:192 now
where the time goes in v10:
time: 35.8 us; the launch traced here: 35.5 us
  Pallas kernels  34.8 us (97%)
  local copies, waits for them, and re-layouts  0.63 us (2%)
    pallas_call x1, Pallas kernels, on_device(): pl.pallas_call(kernel, out_shape=jax.ShapeDtypeStruct((64, 512), BF16), i...  34.8 us

profile of v10, /device:TPU:192, one launch (start us, length us, event | category | flops | bytes accessed | tf_op | source)
XLA Modules:
  0.0 35.5 jit_solution(6507753041642725673)
XLA Ops:
  0.0 34.8 %shard_map.163 = bf16[64,512]{1,0:T(8,128)(2,1)S(1)} custom-call(bf16[16,2048]{1,0:T(8,128)(2,1)} %hidden_hbm.1, f32[1,2048]{1,0:T(1,128)} %bitcast.5, bf16[2048,256]{1,0:T(8,128)(2,1)} %w_query.1, bf16[2048,256]{1,0:T(8,128)(2,1)} %w_key.1, bf16[2048,256]{1,0:T(8,128)(2,1)} %w_value.1, f32[2]{0:T(128)} %offset_hbm.1, bf16[2048,256]{1,0:T(8,128)(2,1)} %w_a.1, ...), custom_call_target="tpu_custom_call" | custom-call | tf_op jit(solution)/shard_map/pallas_call | solution.py:533
  34.8 0.6 %copy.19 = bf16[64,512]{1,0:T(8,128)(2,1)} copy(bf16[64,512]{1,0:T(8,128)(2,1)S(1)} %shard_map.163) | data formatting | bytes 131072

commit v11 on v10

--- a/solution.py
+++ b/solution.py
@@ -382,7 +382,7 @@
     def _():
         some_blocks((2, 5))
 
-    relay(1, high=5)
+    relay(1, high=6)
     blocks(6, 7)
     blocks(3, 4)
 
@@ -390,7 +390,7 @@
         start(rc(tbl, tblr.at[x], t_s, t_r, dev(xx=xpeer(d))))
     tblr[x] = tbl[...]
 
-    relay(1, low=5)
+    relay(1, low=6)
     srx[y] = stx[...]
     came(*all_st)
     stats = [srx[i] for i in range(NY)]
@@ -408,12 +408,15 @@
         yy = ypeer(d)
         start(rc(cst.at[yy], crx.at[y], c_s, c_r, dev(yy=yy)))
 
-    for k in (0, 1, 2, 7, 6, 5, 3, 4):
-        @pl.when(z >= k)
-        def _():
-            come(1, k)
-            row = zpeer(-k)
-            obuf[row] = dot(stk[k], vbuf[row])
+    def values(ks):
+        for k in ks:
+            @pl.when(z >= k)
+            def _():
+                come(1, k)
+                row = zpeer(-k)
+                obuf[row] = dot(stk[k], vbuf[row])
+
+    values((0, 1, 2, 7, 6, 5))
 
     came(*all_t)
 
@@ -429,19 +432,20 @@
     per_row = weight.T
     for b in range(NX):
         wbuf[b] = per_row[b * HD : (b + 1) * HD, :]
-    for d in (2, 1, 3, 0):
-        b = xpeer(d)
-        per_row = wbuf[b]
-        rows = pl.ds(pl.multiple_of(b * HD, HD), HD)
-        acc = obuf[0, rows, :] * per_row[:, 0:1]
-        for j in range(1, NZ):
-            acc = acc + obuf[j, rows, :] * per_row[:, j : j + 1]
-        if d > 0:
-            ps[d] = acc.astype(BF16)
-        else:
-            own[...] = acc
+    values((3, 4))
     halves = [slice(i * 64, (i + 1) * 64) for i in (0, 1)]
     for i in (0, 1):
+        for d in (2, 1, 3, 0):
+            b = xpeer(d)
+            per_row = wbuf[b, halves[i], :]
+            rows = pl.ds(pl.multiple_of(b * HD + i * 64, 64), 64)
+            acc = obuf[0, rows, :] * per_row[:, 0:1]
+            for j in range(1, NZ):
+                acc = acc + obuf[j, rows, :] * per_row[:, j : j + 1]
+            if d > 0:
+                ps[d, halves[i], :] = acc.astype(BF16)
+            else:
+                own[halves[i], :] = acc
         for d in (2, 1, 3):
             start(rc(ps.at[d, halves[i]], pr.at[x, halves[i]], o_s.at[i], o_r.at[i], dev(xx=xpeer(d))))
 

time: 35.8 us -> 35.5 us (level)
  no operation moved by 1% of the time
where the time goes in v11:
time: 35.5 us; the launch traced here: 35.1 us
  Pallas kernels  34.5 us (97%)
  local copies, waits for them, and re-layouts  0.63 us (2%)
    pallas_call x1, Pallas kernels, on_device(): pl.pallas_call(kernel, out_shape=jax.ShapeDtypeStruct((64, 512), BF16), i...  34.5 us

profile of v11, /device:TPU:192, one launch (start us, length us, event | category | flops | bytes accessed | tf_op | source)
XLA Modules:
  0.0 35.1 jit_solution(15289249652532437307)
XLA Ops:
  0.0 34.5 %shard_map.163 = bf16[64,512]{1,0:T(8,128)(2,1)S(1)} custom-call(bf16[16,2048]{1,0:T(8,128)(2,1)} %hidden_hbm.1, f32[1,2048]{1,0:T(1,128)} %bitcast.5, bf16[2048,256]{1,0:T(8,128)(2,1)} %w_query.1, bf16[2048,256]{1,0:T(8,128)(2,1)} %w_key.1, bf16[2048,256]{1,0:T(8,128)(2,1)} %w_value.1, f32[2]{0:T(128)} %offset_hbm.1, bf16[2048,256]{1,0:T(8,128)(2,1)} %w_a.1, ...), custom_call_target="tpu_custom_call" | custom-call | tf_op jit(solution)/shard_map/pallas_call | solution.py:537
  34.5 0.6 %copy.19 = bf16[64,512]{1,0:T(8,128)(2,1)} copy(bf16[64,512]{1,0:T(8,128)(2,1)S(1)} %shard_map.163) | data formatting | bytes 131072

commit v12 on v11

--- a/solution.py
+++ b/solution.py
@@ -234,7 +234,7 @@
         tables[h][z, my64, :] = both[:, HD:]
         if h == 0:
             z_own(h, 0)
-            z_own(h, 1)
+            z_own(h, 1, c == 0)
         else:
             z_own(h, 0, c == 0)
 
@@ -253,6 +253,7 @@
         if d > 0:
             start(rc(mine, mine, q_s, q_r, dev(xx=xpeer(d))))
 
+    z_own(0, 1, c == 1)
     project(1)
     local[C_A].wait()
     local[C_B].wait()

time: 35.5 us -> 35.5 us (level)
  no operation moved by 1% of the time
where the time goes in v12:
time: 35.5 us; the launch traced here: 35.2 us
  Pallas kernels  34.5 us (97%)
  local copies, waits for them, and re-layouts  0.63 us (2%)
    pallas_call x1, Pallas kernels, on_device(): pl.pallas_call(kernel, out_shape=jax.ShapeDtypeStruct((64, 512), BF16), i...  34.5 us

profile of v12, /device:TPU:192, one launch (start us, length us, event | category | flops | bytes accessed | tf_op | source)
XLA Modules:
  0.0 35.2 jit_solution(4967724053891898393)
XLA Ops:
  0.0 34.5 %shard_map.163 = bf16[64,512]{1,0:T(8,128)(2,1)S(1)} custom-call(bf16[16,2048]{1,0:T(8,128)(2,1)} %hidden_hbm.1, f32[1,2048]{1,0:T(1,128)} %bitcast.5, bf16[2048,256]{1,0:T(8,128)(2,1)} %w_query.1, bf16[2048,256]{1,0:T(8,128)(2,1)} %w_key.1, bf16[2048,256]{1,0:T(8,128)(2,1)} %w_value.1, f32[2]{0:T(128)} %offset_hbm.1, bf16[2048,256]{1,0:T(8,128)(2,1)} %w_a.1, ...), custom_call_target="tpu_custom_call" | custom-call | tf_op jit(solution)/shard_map/pallas_call | solution.py:538
  34.5 0.6 %copy.19 = bf16[64,512]{1,0:T(8,128)(2,1)} copy(bf16[64,512]{1,0:T(8,128)(2,1)S(1)} %shard_map.163) | data formatting | bytes 131072
